TPU v7x, 256 devices: a whole 4x4x8 slice. The times are simulated.
256 devices in a mesh: ep: 16 (over y, x), tp: 16 (over z, core).
Axes of the slice: x: 4, y: 4, z: 8, core: 2. Of those that a mesh axis runs over, the one named last changes fastest.
Arguments:
- layer_in: bfloat16 [512, 2048], P('ep'), may hold values from -6 to 6
- attn_gain: float32 [2048], replicated, may hold values from 0.1 to 1.9
- query_weight: bfloat16 [2048, 1024], P(None, 'tp'), may hold values from -0.125 to 0.125
- key_weight: bfloat16 [2048, 1024], P(None, 'tp'), may hold values from -0.125 to 0.125
- value_weight: bfloat16 [2048, 1024], P(None, 'tp'), may hold values from -0.125 to 0.125
- forget_weight: bfloat16 [2048, 16], replicated, may hold values from -0.125 to 0.125
- forget_bias: float32 [16], replicated, may hold values from -2 to 3
- out_weight: bfloat16 [1024, 2048], P('tp'), may hold values from -0.1875 to 0.1875
- kv_cache: bfloat16 [512, 16, 1024, 128], P('ep', 'tp'), may hold values from -110 to 110
- cum_gates: float32 [512, 16, 1024], P('ep', 'tp'), may hold values from -144 to 0, as said below
- lengths: int32 [512], P('ep'), may hold values from 512 to 1024, as said below
- ffn_gain: float32 [2048], replicated, may hold values from 0.1 to 1.9
- route_ids: int32 [512, 6], P('ep'), may hold values from 0 to 127, all different within a row; in each aligned block of 32 rows (0 to 31, 32 to 63, ...) at most 2 rows name the same one
- route_weights: float32 [512, 6], P('ep'), may hold values from 0.1 to 1
- shared_gate: bfloat16 [2048, 512], P(None, 'tp'), may hold values from -0.125 to 0.125
- shared_up: bfloat16 [2048, 512], P(None, 'tp'), may hold values from -0.125 to 0.125
- shared_down: bfloat16 [512, 2048], P('tp'), may hold values from -0.25 to 0.25
- expert_gate: bfloat16 [256, 2048, 256], P(('ep', 'tp')), may hold values from -0.125 to 0.125
- expert_up: bfloat16 [256, 2048, 256], P(('ep', 'tp')), may hold values from -0.125 to 0.125
- expert_down: bfloat16 [256, 256, 2048], P(('ep', 'tp')), may hold values from -0.25 to 0.25
Outputs:
- layer_out: bfloat16 [512, 2048], P('ep')
- new_kv: bfloat16 [512, 16, 128], P('ep', 'tp')
Inputs may be any that keep to these rules, and one draw needn't show every extreme that they name: `cum_gates`: never rising along positions. `lengths`: every length is at most 1024, and some sequence's length is exactly 1024. `route_ids`: each row names 6 different experts. Among the 32 rows of one index of ep (aligned blocks), no expert is named by more than 2 rows, and in some block one expert is named by exactly 2 rows.
All inputs are finite; a program needn't handle non-finite values.
Results may differ from a plain program's by a relative error of at most 0.019.
Values may be sent and summed in bfloat16 or wider, within the bound.
No kernel may reach another device: no remote copies, remote signals or barrier semaphores. Data moves between devices by JAX's collectives and lax.ppermute only.
A program may use at most 64 MiB of HBM per device.

v0:
```python
import jax
import jax.numpy as jnp
from jax import lax
from jax.sharding import PartitionSpec as P

NORM_EPS = 1e-06


def cut_along(shard, dim, peers):
    before, after = (shard.shape[:dim], shard.shape[dim + 1 :])
    return jnp.moveaxis(shard.reshape(*before, peers, -1, *after), dim, 0)


def summed_on_arrival(shard, axis, dim):
    tiles = cut_along(shard, dim, lax.axis_size(axis))
    arrived = lax.all_to_all(tiles, axis, split_axis=0, concat_axis=0, tiled=True)
    return arrived.astype(jnp.float32).sum(axis=0)


def in_one_piece(arrays, axis, dim, along):
    both = jnp.concatenate(arrays, axis=along)
    filled, at, outs = (lax.all_gather(both, axis, axis=dim, tiled=True), 0, [])
    for a in arrays:
        outs.append(lax.slice_in_dim(filled, at, at + a.shape[along], axis=along))
        at += a.shape[along]
    return tuple(outs)


def rms_scale(stream, gain):
    wide = stream.astype(jnp.float32)
    factor = lax.rsqrt(jnp.mean(wide * wide, axis=-1, keepdims=True) + NORM_EPS)
    return (wide * factor * gain).astype(jnp.bfloat16)


def project(normed, weight):
    return jnp.dot(normed, weight, preferred_element_type=jnp.float32).astype(jnp.bfloat16)


def attend(queries, new_key, new_value, forget, kv_block, cum_block, length_block):
    head_size = queries.shape[-1]
    cache_span = kv_block.shape[2]
    positions = jnp.arange(cache_span, dtype=jnp.int32)
    inside = positions[None, None, :] < length_block[:, None, None]
    at_last = positions[None, None, :] == (length_block - 1)[:, None, None]
    latest = jnp.sum(jnp.where(at_last, cum_block, 0.0), axis=-1)
    scaling = head_size ** (-0.5)
    cached_keys = kv_block[..., :head_size]
    cached_values = kv_block[..., head_size:]
    scores = (
        jnp.einsum("shd,shld->shl", queries, cached_keys, preferred_element_type=jnp.float32)
        * scaling
    )
    scores = jnp.where(inside, scores + (latest + forget)[..., None] - cum_block, -jnp.inf)
    itself = jnp.sum(queries.astype(jnp.float32) * new_key.astype(jnp.float32), axis=-1) * scaling
    highest = jnp.maximum(jnp.max(scores, axis=-1), itself)
    earlier = jnp.exp(scores - highest[..., None])
    own_term = jnp.exp(itself - highest)
    denominator = jnp.sum(earlier, axis=-1) + own_term
    past_probs = (earlier / denominator[..., None]).astype(jnp.bfloat16)
    own_probs = (own_term / denominator).astype(jnp.bfloat16)
    blended = jnp.einsum(
        "shl,shld->shd", past_probs, cached_values, preferred_element_type=jnp.float32
    )
    blended = blended + own_probs.astype(jnp.float32)[..., None] * new_value.astype(jnp.float32)
    return blended.astype(jnp.bfloat16)


def body(
    layer_in,
    attn_gain,
    query_weight,
    key_weight,
    value_weight,
    forget_weight,
    forget_bias,
    out_weight,
    kv_cache,
    cum_gates,
    lengths,
    ffn_gain,
    route_ids,
    route_weights,
    shared_gate,
    shared_up,
    shared_down,
    expert_gate,
    expert_up,
    expert_down,
):
    row_count = layer_in.shape[0]
    width = layer_in.shape[1]
    heads_here = kv_cache.shape[1]
    head_size = kv_cache.shape[3] // 2
    normed = rms_scale(layer_in, attn_gain)
    queries = project(normed, query_weight).reshape(row_count, heads_here, head_size)
    new_key = project(normed, key_weight).reshape(row_count, heads_here, head_size)
    new_value = project(normed, value_weight).reshape(row_count, heads_here, head_size)
    new_kv = jnp.concatenate([new_key, new_value], axis=-1)
    first_head = lax.axis_index("tp") * heads_here
    gate_logits = jnp.dot(normed, forget_weight, preferred_element_type=jnp.float32) + forget_bias
    forget = jax.nn.log_sigmoid(lax.dynamic_slice_in_dim(gate_logits, first_head, heads_here, 1))
    attended = attend(queries, new_key, new_value, forget, kv_cache, cum_gates, lengths)
    head_part = jnp.dot(
        attended.reshape(row_count, heads_here * head_size),
        out_weight,
        preferred_element_type=jnp.float32,
    )
    slice_rows = row_count // lax.axis_size("tp")
    slice_start = lax.axis_index("tp") * slice_rows
    head_slice = summed_on_arrival(head_part.astype(jnp.bfloat16), "tp", 0)
    own_stream = lax.dynamic_slice_in_dim(layer_in, slice_start, slice_rows, 0)
    middle_slice = (own_stream.astype(jnp.float32) + head_slice).astype(jnp.bfloat16)
    hidden_slice = rms_scale(middle_slice, ffn_gain)
    middle, hidden_in = in_one_piece((middle_slice, hidden_slice), "tp", 0, 1)
    shared_hidden = (
        jax.nn.silu(jnp.dot(hidden_in, shared_gate, preferred_element_type=jnp.float32))
        * jnp.dot(hidden_in, shared_up, preferred_element_type=jnp.float32)
    ).astype(jnp.bfloat16)
    shared_part = jnp.dot(shared_hidden, shared_down, preferred_element_type=jnp.float32)
    my_gate = expert_gate[0]
    my_up = expert_up[0]
    my_down = expert_down[0]
    ep_count = lax.axis_size("ep")
    pair_count = lax.axis_size("tp") // 2
    column = lax.axis_index("tp") // 2
    picks = route_ids.shape[1]
    experts = ep_count * pair_count
    capacity = max(2, 4 * row_count * picks // (3 * experts))
    targets = jnp.arange(ep_count, dtype=jnp.int32) * pair_count + column
    matches = route_ids[:, :, None] == targets[None, None, :]
    member = jnp.any(matches, axis=1).astype(jnp.int32)
    weight = jnp.sum(jnp.where(matches, route_weights[:, :, None], 0.0), axis=1)
    ranking = jnp.cumsum(member, axis=0) - member
    slot_numbers = jnp.arange(capacity, dtype=jnp.int32)
    placement = (member[:, :, None] == 1) & (ranking[:, :, None] == slot_numbers[None, None, :])
    dispatch = jnp.einsum(
        "rs,rd->sd",
        placement.reshape(row_count, ep_count * capacity).astype(jnp.bfloat16),
        hidden_in,
        preferred_element_type=jnp.float32,
    ).astype(jnp.bfloat16)
    dispatch = dispatch.reshape(ep_count, capacity, width)
    received = lax.all_to_all(dispatch, "ep", split_axis=0, concat_axis=0, tiled=True)
    count = received.shape[1]
    batch_rows = received.reshape(ep_count * count, width)
    hidden = (
        jax.nn.silu(jnp.dot(batch_rows, my_gate, preferred_element_type=jnp.float32))
        * jnp.dot(batch_rows, my_up, preferred_element_type=jnp.float32)
    ).astype(jnp.bfloat16)
    served = jnp.dot(hidden, my_down, preferred_element_type=jnp.float32).reshape(
        ep_count, count, width
    )
    returned = lax.all_to_all(
        served.astype(jnp.bfloat16), "ep", split_axis=0, concat_axis=0, tiled=True
    ).astype(served.dtype)
    shares = (placement.astype(jnp.float32) * weight[:, :, None]).reshape(
        row_count, ep_count * capacity
    )
    routed = jnp.dot(
        shares,
        returned.reshape(ep_count * capacity, width),
        precision=lax.Precision.HIGHEST,
        preferred_element_type=jnp.float32,
    )
    mixed_slice = summed_on_arrival((shared_part + routed).astype(jnp.bfloat16), "tp", 0)
    own_middle = lax.dynamic_slice_in_dim(middle, slice_start, slice_rows, 0)
    out_slice = (own_middle.astype(jnp.float32) + mixed_slice).astype(jnp.bfloat16)
    layer_out = lax.all_gather(out_slice, "tp", axis=0, tiled=True)
    return (layer_out, new_kv)


def solution(mesh):
    placed = (
        P("ep", None),
        P(),
        P(None, "tp"),
        P(None, "tp"),
        P(None, "tp"),
        P(),
        P(),
        P("tp", None),
        P("ep", "tp", None, None),
        P("ep", "tp", None),
        P("ep"),
        P(),
        P("ep", None),
        P("ep", None),
        P(None, "tp"),
        P(None, "tp"),
        P("tp", None),
        P(("ep", "tp"), None, None),
        P(("ep", "tp"), None, None),
        P(("ep", "tp"), None, None),
    )
    return jax.shard_map(
        body,
        mesh=mesh,
        in_specs=placed,
        out_specs=(P("ep", None), P("ep", "tp", None)),
        check_vma=False,
    )
```

profile of v0, /device:TPU:1, one launch (start us, length us, event | category | flops | bytes accessed | tf_op | source)
XLA Modules:
  0.0 121.0 jit_solution(8280109137043809349)
XLA Ops:
  0.7 1.1 fusion.13
  2.5 1.1 fusion.55
  3.7 1.3 %convolution_convert_fusion.5 = bf16[32,64]{1,0:T(8,128)(2,1)S(1)} fusion(bf16[2048,64]{0,1:T(8,128)(2,1)} %param.22, bf16[32,2048]{1,0:T(8,128)(2,1)} %param.20, f32[2048]{0:T(1024)} %param.21, f32[32]{0:T(128)S(1)} %add_rsqrt_fusion.1), kind=kOutput, calls=%fused_computation.18 | convolution fusion | flops 8652800 | bytes 405632 | tf_op jit(solution)/shard_map/dot_general | solution.py:36
  5.0 1.4 %dynamic-slice = f32[1]{0:T(128)} dynamic-slice(f32[16]{0:T(128)} %param.26, s32[]{:T(128)S(6)} %select_n.30), dynamic_slice_sizes={1} | dynamic-slice | bytes 12 | tf_op jit(solution)/shard_map/dynamic_slice | solution.py:101
  6.4 1.8 %fusion.21 = f32[32]{0:T(128)S(1)} fusion(f32[32,1,1024]{2,1,0:T(1,128)} %param.29, s32[32]{0:T(128)S(1)} %broadcast_add_fusion), kind=kLoop, calls=%fused_computation.39 | loop fusion | flops 98272 | bytes 131328 | tf_op jit(solution)/shard_map/reduce_sum | solution.py:45
  8.1 5.6 %fusion.2 = f32[32,1,1024]{2,1,0:T(1,128)S(1)} fusion(bf16[32,1,1024,128]{3,2,1,0:T(8,128)(2,1)} %param.28, bf16[32,64,1]{1,0,2:T(8,128)(2,1)S(1)} %bitcast.54), kind=kOutput, calls=%fused_computation.2 | convolution fusion | flops 4194304 | bytes 8523776 | tf_op jit(solution)/shard_map/shd,shld->shl/dot_general | solution.py:50
  15.2 1.0 multiply_reduce_fusion
  16.8 2.6 %fusion = f32[32,1,64]{2,1,0:T(1,128)S(1)} fusion(bf16[32,1,1024,128]{3,2,1,0:T(8,128)(2,1)S(1)} %copy-done.1, f32[32]{0:T(128)S(1)} %get-tuple-element.9, f32[32,1,1024]{2,1,0:T(1,128)S(1)} %get-tuple-element.5, f32[32]{0:T(128)S(1)} %multiply_maximum_fusion), kind=kOutput, calls=%fused_computation | convolution fusion | flops 4292608 | bytes 8528128 | tf_op jit(solution)/shard_map/shl,shld->shd/dot_general | solution.py:61
  20.7 10.0 %all-to-all-start = ((bf16[16,2,2048]{2,1,0:T(2,128)(2,1)}), bf16[16,2,2048]{2,1,0:T(2,128)(2,1)S(1)}, u32[]{:S(2)}, u32[]{:S(2)}) async-start(bf16[16,2,2048]{2,1,0:T(2,128)(2,1)} %reshape.219), calls=%async_computation | async-start | bytes 262144 | tf_op jit(solution)/shard_map/all_to_all | solution.py:16
  33.1 6.5 %all-to-all-done = bf16[16,2,2048]{2,1,0:T(2,128)(2,1)S(1)} async-done(((bf16[16,2,2048]{2,1,0:T(2,128)(2,1)}), bf16[16,2,2048]{2,1,0:T(2,128)(2,1)S(1)}, u32[]{:S(2)}, u32[]{:S(2)}) %all-to-all-start) | async-done | bytes 131104 | tf_op jit(solution)/shard_map/all_to_all | solution.py:16
  39.9 16.6 %all-gather = bf16[16,2,4096]{2,1,0:T(2,128)(2,1)} all-gather(bf16[1,2,4096]{2,1,0:T(2,128)(2,1)S(1)} %maximum_bitcast_fusion), channel_id=1, replica_groups=mesh['ep'=16,'tp'=16] {'tp'}, dimensions={0}, use_global_device_ids=true | all-gather | bytes 278528 | tf_op jit(solution)/shard_map/all_gather | solution.py:22
  56.5 1.0 reshape.226
  59.2 6.8 %all-to-all-start.1 = ((bf16[16,2,2048]{2,1,0:T(2,128)(2,1)}), bf16[16,2,2048]{2,1,0:T(2,128)(2,1)}, u32[]{:S(2)}, u32[]{:S(2)}) async-start(bf16[16,2,2048]{2,1,0:T(2,128)(2,1)} %reshape.220), calls=%async_computation.1 | async-start | bytes 262144 | tf_op jit(solution)/shard_map/all_to_all | solution.py:143
  66.0 1.3 %and_select_fusion = f32[32,16,2]{0,2,1:T(2,128)} fusion(pred[32,16]{0,1:T(8,128)(4,1)} %copy-done.7, f32[32,16]{0,1:T(8,128)} %fusion.28, s32[32,16]{0,1:T(8,128)S(1)} %copy.41), kind=kLoop, calls=%fused_computation.48 | loop fusion | flops 3072 | bytes 8704 | tf_op jit(solution)/shard_map/mul | solution.py:156
  67.4 5.6 %all-to-all-done.1 = bf16[16,2,2048]{2,1,0:T(2,128)(2,1)} async-done(((bf16[16,2,2048]{2,1,0:T(2,128)(2,1)}), bf16[16,2,2048]{2,1,0:T(2,128)(2,1)}, u32[]{:S(2)}, u32[]{:S(2)}) %all-to-all-start.1) | async-done | bytes 131104 | tf_op jit(solution)/shard_map/all_to_all | solution.py:143
  75.6 3.5 %all-to-all-start.2 = ((bf16[16,2,2048]{2,1,0:T(2,128)(2,1)}), bf16[16,2,2048]{2,1,0:T(2,128)(2,1)S(1)}, u32[]{:S(2)}, u32[]{:S(2)}) async-start(bf16[16,2,2048]{2,1,0:T(2,128)(2,1)} %copy.43), calls=%async_computation.2 | async-start | bytes 262144 | tf_op jit(solution)/shard_map/all_to_all | solution.py:153
  79.1 1.1 fusion.25
  80.2 5.7 %all-to-all-done.2 = bf16[16,2,2048]{2,1,0:T(2,128)(2,1)S(1)} async-done(((bf16[16,2,2048]{2,1,0:T(2,128)(2,1)}), bf16[16,2,2048]{2,1,0:T(2,128)(2,1)S(1)}, u32[]{:S(2)}, u32[]{:S(2)}) %all-to-all-start.2) | async-done | bytes 131104 | tf_op jit(solution)/shard_map/all_to_all | solution.py:153
  85.9 1.0 convolution_bitcast_fusion
  87.0 1.3 %fusion.6 = bf16[32,2048]{1,0:T(8,128)(2,1)S(1)} fusion(f32[32,2048]{1,0:T(8,128)S(1)} %convolution_bitcast_fusion, bf16[32,2048]{1,0:T(8,128)(2,1)} %param.36, bf16[2048,32]{0,1:T(8,128)(2,1)} %param.35, bf16[32,4096]{1,0:T(8,128)(2,1)S(1)} %reshape.226, f32[32,32]{1,0:T(8,128)S(1)} %fusion.25), kind=kOutput, calls=%fused_computation.8 | convolution fusion | flops 8525824 | bytes 802816 | tf_op jit(solution)/shard_map/dot_general | solution.py:119
  89.1 7.4 %all-to-all-start.3 = ((bf16[16,2,2048]{2,1,0:T(2,128)(2,1)}), bf16[16,2,2048]{2,1,0:T(2,128)(2,1)S(1)}, u32[]{:S(2)}, u32[]{:S(2)}) async-start(bf16[16,2,2048]{2,1,0:T(2,128)(2,1)} %reshape.222), calls=%async_computation.3 | async-start | bytes 262144 | tf_op jit(solution)/shard_map/all_to_all | solution.py:16
  96.5 1.4 %pad_maximum_fusion = bf16[32,1,128]{2,0,1:T(8,128)(2,1)} fusion(bf16[32,1,64]{2,0,1:T(8,128)(2,1)S(1)} %bitcast.55, bf16[32,1,64]{2,0,1:T(8,128)(2,1)} %bitcast.57), kind=kLoop, calls=%fused_computation.72 | loop fusion | flops 16384 | bytes 16384 | tf_op jit(solution)/shard_map/concatenate | solution.py:98
  97.9 7.5 %all-to-all-done.3 = bf16[16,2,2048]{2,1,0:T(2,128)(2,1)S(1)} async-done(((bf16[16,2,2048]{2,1,0:T(2,128)(2,1)}), bf16[16,2,2048]{2,1,0:T(2,128)(2,1)S(1)}, u32[]{:S(2)}, u32[]{:S(2)}) %all-to-all-start.3) | async-done | bytes 131104 | tf_op jit(solution)/shard_map/all_to_all | solution.py:16
  105.5 14.8 %all-gather.1 = bf16[16,2,2048]{2,1,0:T(2,128)(2,1)S(1)} all-gather(bf16[1,2,2048]{2,1,0:T(2,128)(2,1)S(1)} %fusion.42), channel_id=1, replica_groups=mesh['ep'=16,'tp'=16] {'tp'}, dimensions={0}, use_global_device_ids=true | all-gather | bytes 139264 | tf_op jit(solution)/shard_map/all_gather | solution.py:168
  (73 shorter events, 12.6 us)
Async XLA Ops:
  0.6 73.9 %copy-start = (bf16[1,256,2048]{2,1,0:T(8,128)(2,1)S(1)}, bf16[1,256,2048]{2,1,0:T(8,128)(2,1)}, u32[]{:S(2)}) copy-start(bf16[1,256,2048]{2,1,0:T(8,128)(2,1)} %param.39) | copy-start | bytes 3145732
  0.6 14.6 %copy-start.6 = (bf16[32,2048]{1,0:T(8,128)(2,1)S(1)}, bf16[32,2048]{1,0:T(8,128)(2,1)}, u32[]{:S(2)}) copy-start(bf16[32,2048]{1,0:T(8,128)(2,1)} %param.20) | copy-start | bytes 393220
  0.7 14.0 %copy-start.11 = (s32[32]{0:T(128)S(1)}, s32[32]{0:T(128)}, u32[]{:S(2)}) copy-start(s32[32]{0:T(128)} %param.30) | copy-start | bytes 388
  0.7 14.5 %copy-start.14 = (f32[2048]{0:T(1024)S(1)}, f32[2048]{0:T(1024)}, u32[]{:S(2)}) copy-start(f32[2048]{0:T(1024)} %param.21) | copy-start | bytes 24580
  0.7 14.0 %copy-start.4 = (f32[32,1,1024]{2,1,0:T(1,128)S(1)}, f32[32,1,1024]{2,1,0:T(1,128)}, u32[]{:S(2)}) copy-start(f32[32,1,1024]{2,1,0:T(1,128)} %param.29) | copy-start | bytes 393220
  0.7 14.5 %copy-start.12 = (bf16[2048,64]{0,1:T(8,128)(2,1)S(1)}, bf16[2048,64]{0,1:T(8,128)(2,1)}, u32[]{:S(2)}) copy-start(bf16[2048,64]{0,1:T(8,128)(2,1)} %param.23) | copy-start | bytes 786436
  5.0 11.8 %copy-start.1 = (bf16[32,1,1024,128]{3,2,1,0:T(8,128)(2,1)S(1)}, bf16[32,1,1024,128]{3,2,1,0:T(8,128)(2,1)}, u32[]{:S(2)}) copy-start(bf16[32,1,1024,128]{3,2,1,0:T(8,128)(2,1)} %param.28) | copy-start | bytes 25165828
  13.8 5.6 %copy-start.13 = (bf16[2048,64]{0,1:T(8,128)(2,1)S(1)}, bf16[2048,64]{0,1:T(8,128)(2,1)}, u32[]{:S(2)}) copy-start(bf16[2048,64]{0,1:T(8,128)(2,1)} %param.24) | copy-start | bytes 786436
  13.8 5.9 %copy-start.5 = (bf16[64,2048]{1,0:T(8,128)(2,1)S(1)}, bf16[64,2048]{1,0:T(8,128)(2,1)}, u32[]{:S(2)}) copy-start(bf16[64,2048]{1,0:T(8,128)(2,1)} %param.27) | copy-start | bytes 786436
  13.8 16.9 %copy-start.8 = (s32[32,6]{0,1:T(8,128)S(1)}, s32[32,6]{0,1:T(8,128)}, u32[]{:S(2)}) copy-start(s32[32,6]{0,1:T(8,128)} %param.32) | copy-start | bytes 2308
  13.8 18.6 %copy-start.10 = (f32[32,6]{0,1:T(8,128)S(1)}, f32[32,6]{0,1:T(8,128)}, u32[]{:S(2)}) copy-start(f32[32,6]{0,1:T(8,128)} %param.33) | copy-start | bytes 2308
  13.8 26.0 %copy-start.9 = (f32[2048]{0:T(1024)S(1)}, f32[2048]{0:T(1024)}, u32[]{:S(2)}) copy-start(f32[2048]{0:T(1024)} %param.31) | copy-start | bytes 24580
  15.2 58.7 %copy-start.2 = (bf16[1,2048,256]{2,1,0:T(8,128)(2,1)S(1)}, bf16[1,2048,256]{2,1,0:T(8,128)(2,1)}, u32[]{:S(2)}) copy-start(bf16[1,2048,256]{2,1,0:T(8,128)(2,1)} %param.37) | copy-start | bytes 3145732
  16.8 57.4 %copy-start.3 = (bf16[1,2048,256]{2,1,0:T(8,128)(2,1)S(1)}, bf16[1,2048,256]{2,1,0:T(8,128)(2,1)}, u32[]{:S(2)}) copy-start(bf16[1,2048,256]{2,1,0:T(8,128)(2,1)} %param.38) | copy-start | bytes 3145732
  20.7 18.9 %all-to-all-start = ((bf16[16,2,2048]{2,1,0:T(2,128)(2,1)}), bf16[16,2,2048]{2,1,0:T(2,128)(2,1)S(1)}, u32[]{:S(2)}, u32[]{:S(2)}) async-start(bf16[16,2,2048]{2,1,0:T(2,128)(2,1)} %reshape.219), calls=%async_computation | async-start | bytes 262144 | tf_op jit(solution)/shard_map/all_to_all | solution.py:16
  31.1 2.0 %copy-start.7 = (pred[32,16]{0,1:T(8,128)(4,1)}, pred[32,16]{0,1:T(8,128)(4,1)S(1)}, u32[]{:S(2)}) copy-start(pred[32,16]{0,1:T(8,128)(4,1)S(1)} %copy.40) | copy-start | bytes 1540
  59.2 13.7 %all-to-all-start.1 = ((bf16[16,2,2048]{2,1,0:T(2,128)(2,1)}), bf16[16,2,2048]{2,1,0:T(2,128)(2,1)}, u32[]{:S(2)}, u32[]{:S(2)}) async-start(bf16[16,2,2048]{2,1,0:T(2,128)(2,1)} %reshape.220), calls=%async_computation.1 | async-start | bytes 262144 | tf_op jit(solution)/shard_map/all_to_all | solution.py:143
  75.6 10.3 %all-to-all-start.2 = ((bf16[16,2,2048]{2,1,0:T(2,128)(2,1)}), bf16[16,2,2048]{2,1,0:T(2,128)(2,1)S(1)}, u32[]{:S(2)}, u32[]{:S(2)}) async-start(bf16[16,2,2048]{2,1,0:T(2,128)(2,1)} %copy.43), calls=%async_computation.2 | async-start | bytes 262144 | tf_op jit(solution)/shard_map/all_to_all | solution.py:153
  89.1 16.3 %all-to-all-start.3 = ((bf16[16,2,2048]{2,1,0:T(2,128)(2,1)}), bf16[16,2,2048]{2,1,0:T(2,128)(2,1)S(1)}, u32[]{:S(2)}, u32[]{:S(2)}) async-start(bf16[16,2,2048]{2,1,0:T(2,128)(2,1)} %reshape.222), calls=%async_computation.3 | async-start | bytes 262144 | tf_op jit(solution)/shard_map/all_to_all | solution.py:16
where the time goes:
time: 122 us; the launch traced here: 121 us
  blocking collectives  31.4 us (26%)
  starting transfers between devices  27.7 us (23%)
  waiting for transfers between devices  25.3 us (21%)
  matrix products  17.3 us (14%)
  other arithmetic  9.49 us (8%)
  local copies, waits for them, and re-layouts  8.9 us (7%)
    all_to_all x2, starting transfers between devices, summed_on_arrival(): lax.all_to_all(tiles, axis, split_axis=0, concat_axis=0, tiled=True)  17.4 us
    all_gather x1, blocking collectives, in_one_piece(): filled, at, outs = (lax.all_gather(both, axis, axis=dim, tiled=True), 0, [])  16.6 us
    all_gather x1, blocking collectives, body(): layer_out = lax.all_gather(out_slice, 'tp', axis=0, tiled=True)  14.8 us
    all_to_all x2, waiting for transfers between devices, summed_on_arrival(): lax.all_to_all(tiles, axis, split_axis=0, concat_axis=0, tiled=True)  14 us
    all_to_all x1, starting transfers between devices, body(): lax.all_to_all(dispatch, 'ep', split_axis=0, concat_axis=0, tiled=True)  6.8 us
    all_to_all x1, waiting for transfers between devices, body(): lax.all_to_all(served.astype(jnp.bfloat16), 'ep', split_axis=0, concat_ax...  5.74 us
    dot_general x1, matrix products, attend(): jnp.einsum('shd,shld->shl', queries, cached_keys, preferred_element_type=...  5.63 us
    all_to_all x1, waiting for transfers between devices, body(): lax.all_to_all(dispatch, 'ep', split_axis=0, concat_axis=0, tiled=True)  5.58 us
  transfers between devices with their start and end apart: 4, of which 4 were waited for; matrix products, arithmetic and copies ran while one was open for 5% of the time, Pallas kernels for 0%

commit v1 on v0

v1 whole, which is shorter than its diff:
```python
import functools

import jax
import jax.numpy as jnp
from jax import lax
from jax.experimental import pallas as pl
from jax.experimental.pallas import tpu as pltpu
from jax.sharding import Mesh, PartitionSpec as P

NORM_EPS = 1e-06
BF = jnp.bfloat16
F32 = jnp.float32
LANES = 128
VMEM = pltpu.VMEM
EP = ("y", "x")
TP = ("z", "c")
ALL = ("y", "x", "z", "c")


def nt(a, b):
    return lax.dot_general(a, b, (((1,), (1,)), ((), ())), preferred_element_type=F32)


def tn(a, b):
    return lax.dot_general(a, b, (((0,), (0,)), ((), ())), preferred_element_type=F32)


def mm(a, b):
    return jnp.dot(a, b, preferred_element_type=F32)


def rms_rows(wide, gain):
    factor = lax.rsqrt(jnp.mean(wide * wide, axis=-1, keepdims=True) + NORM_EPS)
    return (wide * factor * gain).astype(BF)


def attention_kernel(
    lengths_ref,
    bias_ref,
    head_ref,
    layer_ref,
    gain_ref,
    wq_ref,
    wk_ref,
    wv_ref,
    wf_ref,
    wo_ref,
    cum_ref,
    kv_hbm,
    part_ref,
    newkv_ref,
    kv_buf,
    sems,
):
    rows, width = layer_ref.shape
    span = kv_hbm.shape[2]
    hd = wq_ref.shape[0]
    copies = [
        pltpu.make_async_copy(
            kv_hbm.at[s, 0], kv_buf.at[:, s * LANES : (s + 1) * LANES], sems.at[s]
        )
        for s in range(rows)
    ]
    for copy in copies:
        copy.start()

    normed = rms_rows(layer_ref[...].astype(F32), gain_ref[...])
    padded = jnp.concatenate([normed, jnp.zeros((LANES - rows, width), BF)], axis=0)
    stacked = jnp.concatenate([wq_ref[...], wk_ref[...], wf_ref[...]], axis=0)
    by_seq = nt(stacked, padded)
    query = by_seq[:hd].astype(BF).astype(F32)
    key = by_seq[hd : 2 * hd].astype(BF).astype(F32)
    new_kv = nt(normed, jnp.concatenate([wk_ref[...], wv_ref[...]], axis=0)).astype(BF)
    newkv_ref[...] = new_kv

    scaling = hd ** (-0.5)
    query = query * scaling
    itself = jnp.sum(query * key, axis=0, keepdims=True)
    head = head_ref[0]
    head_row = lax.broadcasted_iota(jnp.int32, (wf_ref.shape[0], LANES), 0) == head
    logit = (
        jnp.sum(jnp.where(head_row, by_seq[2 * hd :], 0.0), axis=0, keepdims=True) + bias_ref[head]
    )
    forget = -(jnp.maximum(-logit, 0.0) + jnp.log1p(jnp.exp(-jnp.abs(logit))))

    lane = lax.broadcasted_iota(jnp.int32, (1, LANES), 1)
    length = jnp.zeros((1, LANES), jnp.int32)
    for s in range(rows):
        length = jnp.where(lane == s, lengths_ref[s], length)

    cum = cum_ref[...].reshape(rows, span)
    cum = jnp.concatenate([cum, jnp.zeros((LANES - rows, span), F32)], axis=0)
    cum = jnp.transpose(cum)
    position = lax.broadcasted_iota(jnp.int32, (span, LANES), 0)
    latest = jnp.sum(jnp.where(position == length - 1, cum, 0.0), axis=0, keepdims=True)
    shift = (latest + forget) - cum

    query = jnp.concatenate([query, jnp.zeros((LANES - hd, LANES), F32)], axis=0)
    lane_full = lax.broadcasted_iota(jnp.int32, (LANES, LANES), 1)
    scores = shift
    group = 8
    for at in range(0, rows, group):
        spread = jnp.concatenate(
            [jnp.where(lane_full == s, query, 0.0).astype(BF) for s in range(at, at + group)],
            axis=0,
        )
        for s in range(at, at + group):
            copies[s].wait()
        scores = scores + mm(kv_buf[:, at * LANES : (at + group) * LANES], spread)

    scores = jnp.where(position < length, scores, -jnp.inf)
    highest = jnp.maximum(jnp.max(scores, axis=0, keepdims=True), itself)
    earlier = jnp.exp(scores - highest)
    own = jnp.exp(itself - highest)
    inverse = 1.0 / (jnp.sum(earlier, axis=0, keepdims=True) + own)
    probs = jnp.transpose(earlier * inverse)[:rows].astype(BF)
    own = (own * inverse).astype(BF).astype(F32)

    square_row = lax.broadcasted_iota(jnp.int32, (rows, LANES), 0)
    square_lane = lax.broadcasted_iota(jnp.int32, (rows, LANES), 1)
    own_column = jnp.sum(
        jnp.where(square_row == square_lane, own, 0.0), axis=1, keepdims=True
    )
    blended = own_column * new_kv.astype(F32)
    for s in range(rows):
        one = mm(probs, kv_buf[:, s * LANES : (s + 1) * LANES])
        blended = blended + jnp.where(square_row == s, one, 0.0)
    attended = blended[:, hd:].astype(BF)
    out = mm(attended, wo_ref[...])
    for t in range(part_ref.shape[0]):
        part_ref[t] = out[:, t * LANES : (t + 1) * LANES].astype(BF)


def route_kernel(ids_ref, weights_ref, place_ref, high_ref, low_ref):
    picks, rows = ids_ref.shape
    many = place_ref.shape[1]
    square = lax.broadcasted_iota(jnp.int32, (rows, rows), 0) == lax.broadcasted_iota(
        jnp.int32, (rows, rows), 1
    )
    slot = lax.broadcasted_iota(jnp.int32, (rows, many), 1)
    row = lax.broadcasted_iota(jnp.int32, (rows, many), 0)
    expert = slot >> 3
    kind = slot & 3
    weight = jnp.zeros((rows, many), F32)
    member = jnp.zeros((rows, many), F32)
    for k in range(picks):
        ids = ids_ref[k : k + 1, :].astype(F32)
        column = jnp.sum(jnp.where(square, ids, 0.0), axis=1, keepdims=True).astype(jnp.int32)
        share = jnp.sum(jnp.where(square, weights_ref[k : k + 1, :], 0.0), axis=1, keepdims=True)
        match = column == expert
        member = jnp.where(match, 1.0, member)
        weight = jnp.where(match, share, weight)
    earlier = (
        lax.broadcasted_iota(jnp.int32, (rows, rows), 0)
        > lax.broadcasted_iota(jnp.int32, (rows, rows), 1)
    )
    ranking = mm(jnp.where(earlier, 1.0, 0.0).astype(BF), member.astype(BF)).astype(jnp.int32)
    routed = jnp.where(ranking == kind, member, 0.0)
    own = jnp.where(row == ((slot >> 6) * 2 + kind - 2), 1.0, 0.0)
    is_routed = kind < 2
    place_ref[...] = jnp.where(is_routed, routed, own).astype(BF)
    shares = jnp.where(is_routed, routed * weight, own)
    high = shares.astype(BF)
    high_ref[...] = high
    low_ref[...] = (shares - high.astype(F32)).astype(BF)


def middle_kernel(tp_ref, arrived_ref, layer_ref, place_ref, middle_ref, send_ref):
    total = arrived_ref[0].astype(F32)
    for t in range(1, arrived_ref.shape[0]):
        total = total + arrived_ref[t].astype(F32)
    start = pl.multiple_of(tp_ref[0] * LANES, LANES)
    middle = (layer_ref[:, pl.ds(start, LANES)].astype(F32) + total).astype(BF)
    middle_ref[...] = middle
    send_ref[...] = tn(place_ref[...], middle).astype(BF)


def expert_kernel(
    arrived_ref,
    gain_ref,
    gate_ref,
    up_ref,
    down_ref,
    sgate_ref,
    sup_ref,
    sdown_ref,
    send_ref,
    wide_ref,
):
    groups = 16
    kinds = 4
    stride = arrived_ref.shape[0] // groups
    tiles = stride // kinds
    wide_ref[...] = arrived_ref[...].astype(F32)

    def rows_of(s):
        return jnp.concatenate(
            [wide_ref[pl.ds(t * kinds + s, groups, stride=stride), :] for t in range(tiles)],
            axis=1,
        )

    def swish(v):
        return v / (1.0 + jnp.exp(-v))

    gain = gain_ref[...]
    routed = rms_rows(jnp.concatenate([rows_of(0), rows_of(1)], axis=0), gain)
    shared = rms_rows(jnp.concatenate([rows_of(2), rows_of(3)], axis=0), gain)
    hidden = (swish(mm(routed, gate_ref[0])) * mm(routed, up_ref[0])).astype(BF)
    served = mm(hidden, down_ref[0])
    shidden = (swish(nt(shared, sgate_ref[...])) * nt(shared, sup_ref[...])).astype(BF)
    sserved = mm(shidden, sdown_ref[...])
    for s, block in enumerate((served, served, sserved, sserved)):
        for t in range(tiles):
            wide_ref[pl.ds(t * kinds + s, groups, stride=stride), :] = block[
                (s % 2) * groups : (s % 2 + 1) * groups, t * LANES : (t + 1) * LANES
            ]
    send_ref[...] = wide_ref[...].astype(BF)


def combine_kernel(arrived_ref, high_ref, low_ref, middle_ref, send_ref):
    arrived = arrived_ref[...]
    total = mm(high_ref[...], arrived) + mm(low_ref[...], arrived)
    out = (middle_ref[...].astype(F32) + total).astype(BF)
    for t in range(send_ref.shape[0]):
        send_ref[t] = out


def exchange(x, axes):
    return lax.all_to_all(x, axes, split_axis=0, concat_axis=0, tiled=True)


def call(kernel, outs, in_specs=None, scratch=(), **more):
    kw = {} if in_specs is None else {"in_specs": in_specs}
    return pl.pallas_call(
        kernel,
        out_shape=outs,
        scratch_shapes=list(scratch),
        **kw,
        **more,
    )


def body(
    layer_in,
    attn_gain,
    query_weight,
    key_weight,
    value_weight,
    forget_weight,
    forget_bias,
    out_weight,
    kv_cache,
    cum_gates,
    lengths,
    ffn_gain,
    route_ids,
    route_weights,
    shared_gate,
    shared_up,
    shared_down,
    expert_gate,
    expert_up,
    expert_down,
):
    rows, width = layer_in.shape
    span = kv_cache.shape[2]
    tp_count = lax.axis_size(TP)
    everyone = lax.axis_size(ALL)
    tp = lax.axis_index(TP).astype(jnp.int32).reshape(1)
    slots = everyone * 4
    shape = jax.ShapeDtypeStruct
    smem = pl.BlockSpec(memory_space=pltpu.SMEM)
    vmem = pl.BlockSpec(memory_space=pltpu.VMEM)
    hbm = pl.BlockSpec(memory_space=pl.ANY)

    place, high, low = call(
        route_kernel, [shape((rows, slots), BF)] * 3, in_specs=[vmem] * 2
    )(route_ids.T, route_weights.T)
    part, new_kv = call(
        attention_kernel,
        [shape((tp_count, rows, LANES), BF), shape((rows, LANES), BF)],
        in_specs=[smem] * 3 + [vmem] * 8 + [hbm],
        scratch=[pltpu.VMEM((span, rows * LANES), BF), pltpu.SemaphoreType.DMA((rows,))],
    )(
        lengths,
        forget_bias,
        tp,
        layer_in,
        attn_gain.reshape(1, width),
        query_weight.T,
        key_weight.T,
        value_weight.T,
        forget_weight.T,
        out_weight,
        cum_gates,
        kv_cache,
    )
    arrived = exchange(part, TP)
    middle, send = call(
        middle_kernel,
        [shape((rows, LANES), BF), shape((slots, LANES), BF)],
        in_specs=[smem] + [vmem] * 3,
    )(tp, arrived, layer_in, place)
    arrived = exchange(send.reshape(everyone, 4, LANES), ALL).reshape(slots, LANES)
    send = call(
        expert_kernel,
        shape((slots, LANES), BF),
        in_specs=[vmem] * 8,
        scratch=[pltpu.VMEM((slots, LANES), F32)],
    )(
        arrived,
        ffn_gain.reshape(1, width),
        expert_gate,
        expert_up,
        expert_down,
        shared_gate.T,
        shared_up.T,
        shared_down,
    )
    arrived = exchange(send.reshape(everyone, 4, LANES), ALL).reshape(slots, LANES)
    send = call(
        combine_kernel, shape((tp_count, rows, LANES), BF), in_specs=[vmem] * 4
    )(arrived, high, low, middle)
    out = exchange(send, TP)
    layer_out = out.transpose(1, 0, 2).reshape(rows, width)
    return (layer_out, new_kv.reshape(rows, 1, LANES))


def solution(mesh):
    split = Mesh(mesh.devices.reshape(4, 4, 8, 2), ALL)
    placed = (
        P(EP, None),
        P(),
        P(None, TP),
        P(None, TP),
        P(None, TP),
        P(),
        P(),
        P(TP, None),
        P(EP, TP, None, None),
        P(EP, TP, None),
        P(EP),
        P(),
        P(EP, None),
        P(EP, None),
        P(None, TP),
        P(None, TP),
        P(TP, None),
        P(ALL, None, None),
        P(ALL, None, None),
        P(ALL, None, None),
    )
    return jax.shard_map(
        body,
        mesh=split,
        in_specs=placed,
        out_specs=(P(EP, None), P(EP, TP, None)),
        check_vma=False,
    )
```

time: 122 us -> 101 us (0.83)
  blocking collectives: 31.4 us -> 60.3 us
  Pallas kernels: 0 us -> 21.2 us
  waiting for transfers between devices: 25.3 us -> 7.22 us
  starting transfers between devices: 27.7 us -> 9.98 us
  matrix products: 17.3 us -> 0 us
  other arithmetic: 9.49 us -> 0 us
  local copies, waits for them, and re-layouts: 8.9 us -> 1.32 us
    all_to_all x0 -> x3, blocking collectives: none -> 60.3 us  [exchange(): return lax.all_to_all(x, axes, split_axis=0, concat_axis=0, tiled=True)]
    all_gather x2 -> x0, blocking collectives: 31.4 us -> none  [the longest x1 16.6 us: in_one_piece(): filled, at, outs = (lax.all_gather(both, axis, axis=dim, tiled=True), 0, [])]
    pallas_call x0 -> x5, Pallas kernels: none -> 21.2 us  [the longest x1 11.6 us: body(): call(attention_kernel, [shape((tp_count, rows, LANES), BF), shape((rows,...]
    all_to_all x4 -> x1, waiting for transfers between devices: 25.3 us -> 7.22 us  [exchange(): return lax.all_to_all(x, axes, split_axis=0, concat_axis=0, tiled=True)]
    all_to_all x4 -> x1, starting transfers between devices: 27.7 us -> 9.98 us  [exchange(): return lax.all_to_all(x, axes, split_axis=0, concat_axis=0, tiled=True)]
    dot_general x14 -> x0, matrix products: 17.3 us -> none  [the longest x1 5.63 us: attend(): jnp.einsum('shd,shld->shl', queries, cached_keys, preferred_element_type=...]
    reduce_sum x7 -> x0, other arithmetic: 4.48 us -> none  [the longest x1 1.76 us: attend(): latest = jnp.sum(jnp.where(at_last, cum_block, 0.0), axis=-1)]
    reshape x4 -> x1, local copies, waits for them, and re-layouts: 3.24 us -> 0.66 us  [body(): layer_out = out.transpose(1, 0, 2).reshape(rows, width)]
  transfers between devices with their start and end apart: 4 -> 1, of which waited for: 4 -> 1; matrix products, arithmetic and copies ran while one was open for 5% -> 0% of each run, Pallas kernels for 0% -> 2%
where the time goes in v1:
time: 101 us
  blocking collectives  60.3 us (60%)
  Pallas kernels  21.2 us (21%)
  starting transfers between devices  9.98 us (10%)
  waiting for transfers between devices  7.22 us (7%)
  local copies, waits for them, and re-layouts  1.32 us (1%)
    all_to_all x3, blocking collectives, exchange(): return lax.all_to_all(x, axes, split_axis=0, concat_axis=0, tiled=True)  60.3 us
    pallas_call x1, Pallas kernels, body(): call(attention_kernel, [shape((tp_count, rows, LANES), BF), shape((rows,...  11.6 us
    all_to_all x1, starting transfers between devices, exchange(): return lax.all_to_all(x, axes, split_axis=0, concat_axis=0, tiled=True)  9.98 us
    all_to_all x1, waiting for transfers between devices, exchange(): return lax.all_to_all(x, axes, split_axis=0, concat_axis=0, tiled=True)  7.22 us
    pallas_call x1, Pallas kernels, body(): call(expert_kernel, shape((slots, LANES), BF), in_specs=[vmem] * 8, scrat...  4.17 us
  transfers between devices with their start and end apart: 1, of which 1 were waited for; matrix products, arithmetic and copies ran while one was open for 0% of the time, Pallas kernels for 2%

profile of v1, /device:TPU:1, one launch (start us, length us, event | category | flops | bytes accessed | tf_op | source)
XLA Modules:
  0.0 100.7 jit_solution(5225715587411068588)
XLA Ops:
  0.6 11.6 %shard_map.203 = (bf16[16,32,128]{2,1,0:T(8,128)(2,1)}, bf16[32,128]{1,0:T(8,128)(2,1)}) custom-call(s32[32]{0:T(128)} %lengths_ref.1, f32[16]{0:T(128)} %bias_ref.1, s32[1]{0:T(128)} %bitcast.head_ref.tp_ref, bf16[32,2048]{1,0:T(8,128)(2,1)} %layer_ref.3, f32[1,2048]{1,0:T(1,128)} %bitcast.32, bf16[64,2048]{1,0:T(8,128)(2,1)} %bitcast.25, ...), custom_call_target="tpu_custom_call" | custom-call | tf_op jit(solution)/shard_map/pallas_call | solution.py:279
  12.2 10.0 %all-to-all-start = ((bf16[16,32,128]{2,1,0:T(8,128)(2,1)}), bf16[16,32,128]{2,1,0:T(8,128)(2,1)S(1)}, u32[]{:S(2)}, u32[]{:S(2)}) async-start(bf16[16,32,128]{2,1,0:T(8,128)(2,1)} %get-tuple-element.9), calls=%async_computation | async-start | bytes 262144 | tf_op jit(solution)/shard_map/all_to_all | solution.py:229
  22.2 1.7 %shard_map.204 = (bf16[32,1024]{1,0:T(8,128)(2,1)}, bf16[32,1024]{1,0:T(8,128)(2,1)}, bf16[32,1024]{1,0:T(8,128)(2,1)}) custom-call(s32[6,32]{1,0:T(8,128)} %bitcast.34, f32[6,32]{1,0:T(8,128)} %bitcast.35), custom_call_target="tpu_custom_call" | custom-call | tf_op jit(solution)/shard_map/pallas_call | solution.py:276
  23.9 7.2 %all-to-all-done.arrived_ref = bf16[16,32,128]{2,1,0:T(8,128)(2,1)S(1)} async-done(((bf16[16,32,128]{2,1,0:T(8,128)(2,1)}), bf16[16,32,128]{2,1,0:T(8,128)(2,1)S(1)}, u32[]{:S(2)}, u32[]{:S(2)}) %all-to-all-start) | async-done | bytes 131104 | tf_op jit(solution)/shard_map/all_to_all | solution.py:229
  31.1 0.0 copy-start
  31.1 0.7 copy-done
  31.8 1.9 %shard_map.205 = (bf16[32,128]{1,0:T(8,128)(2,1)}, bf16[1024,128]{1,0:T(8,128)(2,1)}) custom-call(s32[1]{0:T(128)} %bitcast.head_ref.tp_ref, bf16[16,32,128]{2,1,0:T(8,128)(2,1)} %copy-done, bf16[32,2048]{1,0:T(8,128)(2,1)} %layer_ref.3, bf16[32,1024]{1,0:T(8,128)(2,1)} %get-tuple-element.10.place_ref), custom_call_target="tpu_custom_call" | custom-call | tf_op jit(solution)/shard_map/pallas_call | solution.py:299
  33.7 24.6 %all_to_all.20 = bf16[256,4,128]{2,1,0:T(4,128)(2,1)} all-to-all(bf16[256,4,128]{2,1,0:T(4,128)(2,1)} %bitcast.28), channel_id=1, replica_groups=mesh['y'=4,'x'=4,'z'=8,'c'=2] {'y','x','z','c'}, dimensions={0} | all-to-all | bytes 524288 | tf_op jit(solution)/shard_map/all_to_all | solution.py:229
  58.2 4.2 %shard_map.206 = bf16[1024,128]{1,0:T(8,128)(2,1)} custom-call(bf16[1024,128]{1,0:T(8,128)(2,1)} %bitcast.22, f32[1,2048]{1,0:T(1,128)} %bitcast.33, bf16[1,2048,256]{2,1,0:T(8,128)(2,1)} %gate_ref.1, bf16[1,2048,256]{2,1,0:T(8,128)(2,1)} %up_ref.1, bf16[1,256,2048]{2,1,0:T(8,128)(2,1)} %down_ref.1, bf16[32,2048]{1,0:T(8,128)(2,1)} %bitcast.29, ...), custom_call_target="tpu_custom_call" | custom-call | tf_op jit(solution)/shard_map/pallas_call | solution.py:305
  62.4 22.8 %all_to_all.21 = bf16[256,4,128]{2,1,0:T(4,128)(2,1)} all-to-all(bf16[256,4,128]{2,1,0:T(4,128)(2,1)} %bitcast.23), channel_id=1, replica_groups=mesh['y'=4,'x'=4,'z'=8,'c'=2] {'y','x','z','c'}, dimensions={0} | all-to-all | bytes 524288 | tf_op jit(solution)/shard_map/all_to_all | solution.py:229
  85.2 1.9 %shard_map.207 = bf16[16,32,128]{2,1,0:T(8,128)(2,1)} custom-call(bf16[1024,128]{1,0:T(8,128)(2,1)} %bitcast.24, bf16[32,1024]{1,0:T(8,128)(2,1)} %get-tuple-element.12.high_ref, bf16[32,1024]{1,0:T(8,128)(2,1)} %get-tuple-element.13.low_ref, bf16[32,128]{1,0:T(8,128)(2,1)} %get-tuple-element.14.middle_ref), custom_call_target="tpu_custom_call" | custom-call | tf_op jit(solution)/shard_map/pallas_call | solution.py:321
  87.0 13.0 %all_to_all.22 = bf16[16,32,128]{2,1,0:T(8,128)(2,1)S(1)} all-to-all(bf16[16,32,128]{2,1,0:T(8,128)(2,1)} %shard_map.207), channel_id=1, replica_groups=mesh['y'=4,'x'=4,'z'=8,'c'=2] {'z','c'}, dimensions={0} | all-to-all | bytes 262144 | tf_op jit(solution)/shard_map/all_to_all | solution.py:229
  100.0 0.7 copy_bitcast_fusion
Async XLA Ops:
  12.2 18.9 %all-to-all-start = ((bf16[16,32,128]{2,1,0:T(8,128)(2,1)}), bf16[16,32,128]{2,1,0:T(8,128)(2,1)S(1)}, u32[]{:S(2)}, u32[]{:S(2)}) async-start(bf16[16,32,128]{2,1,0:T(8,128)(2,1)} %get-tuple-element.9), calls=%async_computation | async-start | bytes 262144 | tf_op jit(solution)/shard_map/all_to_all | solution.py:229
  31.1 0.7 copy-start

commit v2 on v1

--- a/solution.py
+++ b/solution.py
@@ -229,14 +229,13 @@
     return lax.all_to_all(x, axes, split_axis=0, concat_axis=0, tiled=True)
 
 
-def call(kernel, outs, in_specs=None, scratch=(), **more):
-    kw = {} if in_specs is None else {"in_specs": in_specs}
+def call(kernel, outs, in_specs, scratch=(), limit=16 << 20):
     return pl.pallas_call(
         kernel,
         out_shape=outs,
+        in_specs=in_specs,
         scratch_shapes=list(scratch),
-        **kw,
-        **more,
+        compiler_params=pltpu.CompilerParams(vmem_limit_bytes=limit),
     )
 
 
@@ -271,7 +270,7 @@
     shape = jax.ShapeDtypeStruct
     smem = pl.BlockSpec(memory_space=pltpu.SMEM)
     vmem = pl.BlockSpec(memory_space=pltpu.VMEM)
-    hbm = pl.BlockSpec(memory_space=pl.ANY)
+    hbm = pl.BlockSpec(memory_space=pltpu.HBM)
 
     place, high, low = call(
         route_kernel, [shape((rows, slots), BF)] * 3, in_specs=[vmem] * 2
@@ -281,6 +280,7 @@
         [shape((tp_count, rows, LANES), BF), shape((rows, LANES), BF)],
         in_specs=[smem] * 3 + [vmem] * 8 + [hbm],
         scratch=[pltpu.VMEM((span, rows * LANES), BF), pltpu.SemaphoreType.DMA((rows,))],
+        limit=60 * 1024 * 1024,
     )(
         lengths,
         forget_bias,

time: 101 us -> 96.3 us (0.953)
  Pallas kernels: 21.2 us -> 13.9 us
  local copies, waits for them, and re-layouts: 1.32 us -> 6.87 us
  blocking collectives: 60.3 us -> 57.6 us
    unnamed x2 -> x32, local copies, waits for them, and re-layouts: 0.65 us -> 6.2 us
    pallas_call x1, Pallas kernels: 4.17 us -> 1.44 us  [body(): call(expert_kernel, shape((slots, LANES), BF), in_specs=[vmem] * 8, scrat...]
    all_to_all x3, blocking collectives: 60.3 us -> 57.6 us  [exchange(): return lax.all_to_all(x, axes, split_axis=0, concat_axis=0, tiled=True)]
    pallas_call x1, Pallas kernels: 1.93 us -> 0.25 us  [body(): call(middle_kernel, [shape((rows, LANES), BF), shape((slots, LANES), BF)]...]
    pallas_call x1, Pallas kernels: 1.86 us -> 0.21 us  [body(): call(combine_kernel, shape((tp_count, rows, LANES), BF), in_specs=[vmem]...]
    pallas_call x1, Pallas kernels: 1.67 us -> 0.29 us  [body(): call(route_kernel, [shape((rows, slots), BF)] * 3, in_specs=[vmem] * 2)]
  transfers between devices with their start and end apart: 1 -> 1, of which waited for: 1 -> 1; matrix products, arithmetic and copies ran while one was open for 0% -> 0% of each run, Pallas kernels for 2% -> 0%
where the time goes in v2:
time: 96.3 us; the launch traced here: 95.9 us
  blocking collectives  57.6 us (60%)
  Pallas kernels  13.9 us (14%)
  starting transfers between devices  9.98 us (10%)
  local copies, waits for them, and re-layouts  6.87 us (7%)
  waiting for transfers between devices  6.71 us (7%)
    all_to_all x3, blocking collectives, exchange(): return lax.all_to_all(x, axes, split_axis=0, concat_axis=0, tiled=True)  57.6 us
    pallas_call x1, Pallas kernels, body(): call(attention_kernel, [shape((tp_count, rows, LANES), BF), shape((rows,...  11.7 us
    all_to_all x1, starting transfers between devices, exchange(): return lax.all_to_all(x, axes, split_axis=0, concat_axis=0, tiled=True)  9.98 us
    all_to_all x1, waiting for transfers between devices, exchange(): return lax.all_to_all(x, axes, split_axis=0, concat_axis=0, tiled=True)  6.71 us
    unnamed x32, local copies, waits for them, and re-layouts  6.2 us
  transfers between devices with their start and end apart: 1, of which 1 were waited for; matrix products, arithmetic and copies ran while one was open for 0% of the time, Pallas kernels for 0%

profile of v2, /device:TPU:1, one launch (start us, length us, event | category | flops | bytes accessed | tf_op | source)
XLA Modules:
  0.0 95.9 jit_solution(5811548904492996120)
XLA Ops:
  0.6 0.0 copy-start.3
  0.6 0.0 copy-start.15
  0.7 0.0 copy-start.14
  0.7 11.7 %shard_map.203 = (bf16[16,32,128]{2,1,0:T(8,128)(2,1)}, bf16[32,128]{1,0:T(8,128)(2,1)}) custom-call(s32[32]{0:T(128)} %lengths_ref.1, f32[16]{0:T(128)} %bias_ref.1, s32[1]{0:T(128)} %bitcast.head_ref.tp_ref, bf16[32,2048]{1,0:T(8,128)(2,1)} %layer_ref.3, f32[1,2048]{1,0:T(1,128)} %bitcast.35, bf16[64,2048]{1,0:T(8,128)(2,1)} %bitcast.31, ...), custom_call_target="tpu_custom_call" | custom-call | tf_op jit(solution)/shard_map/pallas_call | solution.py:278
  12.5 10.0 %all-to-all-start = ((bf16[16,32,128]{2,1,0:T(8,128)(2,1)}), bf16[16,32,128]{2,1,0:T(8,128)(2,1)S(1)}, u32[]{:S(2)}, u32[]{:S(2)}) async-start(bf16[16,32,128]{2,1,0:T(8,128)(2,1)} %get-tuple-element.9), calls=%async_computation | async-start | bytes 262144 | tf_op jit(solution)/shard_map/all_to_all | solution.py:229
  22.5 0.3 shard_map.204
  22.8 0.6 copy-done.7
  23.4 0.6 copy-done.9
  24.0 0.6 copy-done.11
  24.6 6.7 %all-to-all-done.arrived_ref = bf16[16,32,128]{2,1,0:T(8,128)(2,1)S(1)} async-done(((bf16[16,32,128]{2,1,0:T(8,128)(2,1)}), bf16[16,32,128]{2,1,0:T(8,128)(2,1)S(1)}, u32[]{:S(2)}, u32[]{:S(2)}) %all-to-all-start) | async-done | bytes 131104 | tf_op jit(solution)/shard_map/all_to_all | solution.py:229
  31.3 0.8 copy-done.8
  32.2 0.3 shard_map.205
  32.4 24.2 %all_to_all.20 = bf16[256,4,128]{2,1,0:T(4,128)(2,1)S(1)} all-to-all(bf16[256,4,128]{2,1,0:T(4,128)(2,1)S(1)} %bitcast.25), channel_id=1, replica_groups=mesh['y'=4,'x'=4,'z'=8,'c'=2] {'y','x','z','c'}, dimensions={0} | all-to-all | bytes 524288 | tf_op jit(solution)/shard_map/all_to_all | solution.py:229
  56.7 0.0 copy-done.1
  56.7 0.0 copy-start.5
  56.7 0.9 copy-done.5
  57.6 0.9 copy-done.6
  58.5 1.4 %shard_map.206 = bf16[1024,128]{1,0:T(8,128)(2,1)S(1)} custom-call(bf16[1024,128]{1,0:T(8,128)(2,1)S(1)} %bitcast.22, f32[1,2048]{1,0:T(1,128)S(1)} %bitcast.28, bf16[1,2048,256]{2,1,0:T(8,128)(2,1)S(1)} %copy-done, bf16[1,2048,256]{2,1,0:T(8,128)(2,1)S(1)} %copy-done.1, bf16[1,256,2048]{2,1,0:T(8,128)(2,1)S(1)} %copy-done.2, bf16[32,2048]{1,0:T(8,128)(2,1)S(1)} %bitcast.26, ...), custom_call_target="tpu_custom_call" | custom-call | tf_op jit(solution)/shard_map/pallas_call | solution.py:305
  60.0 21.2 %all_to_all.21 = bf16[256,4,128]{2,1,0:T(4,128)(2,1)S(1)} all-to-all(bf16[256,4,128]{2,1,0:T(4,128)(2,1)S(1)} %bitcast.23), channel_id=1, replica_groups=mesh['y'=4,'x'=4,'z'=8,'c'=2] {'y','x','z','c'}, dimensions={0} | all-to-all | bytes 524288 | tf_op jit(solution)/shard_map/all_to_all | solution.py:229
  81.2 0.8 copy-done.10
  82.1 0.8 copy-done.12
  82.9 0.2 shard_map.207
  83.1 12.1 %all_to_all.22 = bf16[16,32,128]{2,1,0:T(8,128)(2,1)S(1)} all-to-all(bf16[16,32,128]{2,1,0:T(8,128)(2,1)S(1)} %shard_map.207), channel_id=1, replica_groups=mesh['y'=4,'x'=4,'z'=8,'c'=2] {'z','c'}, dimensions={0} | all-to-all | bytes 262144 | tf_op jit(solution)/shard_map/all_to_all | solution.py:229
  95.2 0.7 copy_bitcast_fusion
  (19 shorter events, 0.0 us)
Async XLA Ops:
  0.6 30.7 %copy-start.3 = (bf16[32,2048]{1,0:T(8,128)(2,1)S(1)}, bf16[32,2048]{1,0:T(8,128)(2,1)}, u32[]{:S(2)}) copy-start(bf16[32,2048]{1,0:T(8,128)(2,1)} %layer_ref.3) | copy-start | bytes 393220
  0.6 21.8 %copy-start.15 = (f32[32,6]{0,1:T(8,128)S(1)}, f32[32,6]{0,1:T(8,128)}, u32[]{:S(2)}) copy-start(f32[32,6]{0,1:T(8,128)} %param.33) | copy-start | bytes 2308
  0.7 21.8 %copy-start.14 = (s32[32,6]{0,1:T(8,128)S(1)}, s32[32,6]{0,1:T(8,128)}, u32[]{:S(2)}) copy-start(s32[32,6]{0,1:T(8,128)} %param.32) | copy-start | bytes 2308
  0.7 56.0 %copy-start.2 = (bf16[1,256,2048]{2,1,0:T(8,128)(2,1)S(1)}, bf16[1,256,2048]{2,1,0:T(8,128)(2,1)}, u32[]{:S(2)}) copy-start(bf16[1,256,2048]{2,1,0:T(8,128)(2,1)} %down_ref.1) | copy-start | bytes 3145732
  0.7 56.0 %copy-start.1 = (bf16[1,2048,256]{2,1,0:T(8,128)(2,1)S(1)}, bf16[1,2048,256]{2,1,0:T(8,128)(2,1)}, u32[]{:S(2)}) copy-start(bf16[1,2048,256]{2,1,0:T(8,128)(2,1)} %up_ref.1) | copy-start | bytes 3145732
  0.7 56.0 %copy-start = (bf16[1,2048,256]{2,1,0:T(8,128)(2,1)S(1)}, bf16[1,2048,256]{2,1,0:T(8,128)(2,1)}, u32[]{:S(2)}) copy-start(bf16[1,2048,256]{2,1,0:T(8,128)(2,1)} %gate_ref.1) | copy-start | bytes 3145732
  0.7 56.0 %copy-start.4 = (bf16[2048,32]{0,1:T(8,128)(2,1)S(1)}, bf16[2048,32]{0,1:T(8,128)(2,1)}, u32[]{:S(2)}) copy-start(bf16[2048,32]{0,1:T(8,128)(2,1)} %param.34) | copy-start | bytes 393220
  0.7 56.0 %copy-start.13 = (f32[2048]{0:T(1024)S(1)}, f32[2048]{0:T(1024)}, u32[]{:S(2)}) copy-start(f32[2048]{0:T(1024)} %param.31) | copy-start | bytes 24580
  12.5 18.9 %all-to-all-start = ((bf16[16,32,128]{2,1,0:T(8,128)(2,1)}), bf16[16,32,128]{2,1,0:T(8,128)(2,1)S(1)}, u32[]{:S(2)}, u32[]{:S(2)}) async-start(bf16[16,32,128]{2,1,0:T(8,128)(2,1)} %get-tuple-element.9), calls=%async_computation | async-start | bytes 262144 | tf_op jit(solution)/shard_map/all_to_all | solution.py:229
  22.8 0.6 copy-start.7
  23.4 0.6 copy-start.9
  24.0 0.6 copy-start.11
  31.3 0.8 copy-start.8
  56.7 0.9 copy-start.5
  57.6 0.9 copy-start.6
  81.2 0.8 copy-start.10
  82.0 0.8 copy-start.12

commit v3 on v2

--- a/solution.py
+++ b/solution.py
@@ -35,59 +35,91 @@
 
 
 def attention_kernel(
-    lengths_ref,
-    bias_ref,
+    lengths_hbm,
+    bias_hbm,
     head_ref,
-    layer_ref,
-    gain_ref,
-    wq_ref,
-    wk_ref,
-    wv_ref,
-    wf_ref,
-    wo_ref,
-    cum_ref,
+    layer_hbm,
+    gain_hbm,
+    wq_hbm,
+    wk_hbm,
+    wv_hbm,
+    wf_hbm,
+    wo_hbm,
+    cum_hbm,
     kv_hbm,
     part_ref,
     newkv_ref,
     kv_buf,
+    lengths_ref,
+    bias_ref,
+    layer_ref,
+    gain_ref,
+    first_ref,
+    second_ref,
+    wo_ref,
+    cum_ref,
+    score_ref,
+    kv_sems,
     sems,
 ):
     rows, width = layer_ref.shape
     span = kv_hbm.shape[2]
-    hd = wq_ref.shape[0]
-    copies = [
-        pltpu.make_async_copy(
-            kv_hbm.at[s, 0], kv_buf.at[:, s * LANES : (s + 1) * LANES], sems.at[s]
-        )
-        for s in range(rows)
-    ]
-    for copy in copies:
+    hd = wq_hbm.shape[0]
+    gates = wf_hbm.shape[0]
+    pairs = (
+        (layer_hbm, layer_ref),
+        (gain_hbm, gain_ref),
+        (wq_hbm, first_ref.at[:hd]),
+        (wk_hbm, first_ref.at[hd : 2 * hd]),
+        (wf_hbm, first_ref.at[2 * hd :]),
+        (cum_hbm, cum_ref),
+        (wk_hbm, second_ref.at[:hd]),
+        (wv_hbm, second_ref.at[hd:]),
+        (wo_hbm, wo_ref),
+        (lengths_hbm, lengths_ref),
+        (bias_hbm, bias_ref),
+    )
+    small = [pltpu.make_async_copy(a, b, sems.at[i]) for i, (a, b) in enumerate(pairs)]
+    group = 8
+
+    def fetch(s):
+        at = pl.multiple_of(s * LANES, LANES)
+        return pltpu.make_async_copy(kv_hbm.at[s, 0], kv_buf.at[:, pl.ds(at, LANES)], kv_sems.at[s])
+
+    def start(s, carry):
+        fetch(s).start()
+        return carry
+
+    for copy in small[:6] + small[9:]:
         copy.start()
-
+    lax.fori_loop(0, rows, start, 0)
+
+    for copy in small[:5] + small[9:]:
+        copy.wait()
+    lane = lax.broadcasted_iota(jnp.int32, (1, LANES), 1)
+    length = jnp.zeros((1, LANES), jnp.int32)
+    for s in range(rows):
+        length = jnp.where(lane == s, lengths_ref[s], length)
+
+    for copy in small[6:9]:
+        copy.start()
     normed = rms_rows(layer_ref[...].astype(F32), gain_ref[...])
     padded = jnp.concatenate([normed, jnp.zeros((LANES - rows, width), BF)], axis=0)
-    stacked = jnp.concatenate([wq_ref[...], wk_ref[...], wf_ref[...]], axis=0)
-    by_seq = nt(stacked, padded)
+    by_seq = nt(first_ref[...], padded)
     query = by_seq[:hd].astype(BF).astype(F32)
     key = by_seq[hd : 2 * hd].astype(BF).astype(F32)
-    new_kv = nt(normed, jnp.concatenate([wk_ref[...], wv_ref[...]], axis=0)).astype(BF)
-    newkv_ref[...] = new_kv
 
     scaling = hd ** (-0.5)
     query = query * scaling
     itself = jnp.sum(query * key, axis=0, keepdims=True)
     head = head_ref[0]
-    head_row = lax.broadcasted_iota(jnp.int32, (wf_ref.shape[0], LANES), 0) == head
+    head_row = lax.broadcasted_iota(jnp.int32, (gates, LANES), 0) == head
     logit = (
         jnp.sum(jnp.where(head_row, by_seq[2 * hd :], 0.0), axis=0, keepdims=True) + bias_ref[head]
     )
     forget = -(jnp.maximum(-logit, 0.0) + jnp.log1p(jnp.exp(-jnp.abs(logit))))
 
-    lane = lax.broadcasted_iota(jnp.int32, (1, LANES), 1)
-    length = jnp.zeros((1, LANES), jnp.int32)
-    for s in range(rows):
-        length = jnp.where(lane == s, lengths_ref[s], length)
-
+    small[5].wait()
     cum = cum_ref[...].reshape(rows, span)
     cum = jnp.concatenate([cum, jnp.zeros((LANES - rows, span), F32)], axis=0)
     cum = jnp.transpose(cum)
@@ -97,17 +129,22 @@
 
     query = jnp.concatenate([query, jnp.zeros((LANES - hd, LANES), F32)], axis=0)
     lane_full = lax.broadcasted_iota(jnp.int32, (LANES, LANES), 1)
-    scores = shift
-    group = 8
-    for at in range(0, rows, group):
+    score_ref[...] = shift
+
+    def score_step(j, carry):
+        first = j * group
         spread = jnp.concatenate(
-            [jnp.where(lane_full == s, query, 0.0).astype(BF) for s in range(at, at + group)],
+            [jnp.where(lane_full == first + k, query, 0.0).astype(BF) for k in range(group)],
             axis=0,
         )
-        for s in range(at, at + group):
-            copies[s].wait()
-        scores = scores + mm(kv_buf[:, at * LANES : (at + group) * LANES], spread)
-
+        for k in range(group):
+            fetch(first + k).wait()
+        at = pl.multiple_of(first * LANES, LANES)
+        score_ref[...] += mm(kv_buf[:, pl.ds(at, group * LANES)], spread)
+        return carry
+
+    lax.fori_loop(0, rows // group, score_step, 0)
+    scores = score_ref[...]
     scores = jnp.where(position < length, scores, -jnp.inf)
     highest = jnp.maximum(jnp.max(scores, axis=0, keepdims=True), itself)
     earlier = jnp.exp(scores - highest)
@@ -116,24 +153,36 @@
     probs = jnp.transpose(earlier * inverse)[:rows].astype(BF)
     own = (own * inverse).astype(BF).astype(F32)
 
+    for copy in small[6:9]:
+        copy.wait()
+    new_kv = nt(normed, second_ref[...]).astype(BF)
+    newkv_ref[...] = new_kv
     square_row = lax.broadcasted_iota(jnp.int32, (rows, LANES), 0)
     square_lane = lax.broadcasted_iota(jnp.int32, (rows, LANES), 1)
     own_column = jnp.sum(
         jnp.where(square_row == square_lane, own, 0.0), axis=1, keepdims=True
     )
     blended = own_column * new_kv.astype(F32)
-    for s in range(rows):
-        one = mm(probs, kv_buf[:, s * LANES : (s + 1) * LANES])
-        blended = blended + jnp.where(square_row == s, one, 0.0)
+    step = 8
+
+    def value_step(i, total):
+        for k in range(step):
+            s = (i * step + k) * 2
+            at = pl.multiple_of(s * LANES, LANES)
+            two = mm(probs, kv_buf[:, pl.ds(at, 2 * LANES)])
+            total = total + jnp.where(square_row == s, two[:, :LANES], 0.0)
+            total = total + jnp.where(square_row == s + 1, two[:, LANES:], 0.0)
+        return total
+
+    blended = lax.fori_loop(0, rows // (2 * step), value_step, blended)
     attended = blended[:, hd:].astype(BF)
     out = mm(attended, wo_ref[...])
     for t in range(part_ref.shape[0]):
         part_ref[t] = out[:, t * LANES : (t + 1) * LANES].astype(BF)
 
 
-def route_kernel(ids_ref, weights_ref, place_ref, high_ref, low_ref):
+def routing(ids_ref, weights_ref, many):
     picks, rows = ids_ref.shape
-    many = place_ref.shape[1]
     square = lax.broadcasted_iota(jnp.int32, (rows, rows), 0) == lax.broadcasted_iota(
         jnp.int32, (rows, rows), 1
     )
@@ -146,10 +195,12 @@
     for k in range(picks):
         ids = ids_ref[k : k + 1, :].astype(F32)
         column = jnp.sum(jnp.where(square, ids, 0.0), axis=1, keepdims=True).astype(jnp.int32)
-        share = jnp.sum(jnp.where(square, weights_ref[k : k + 1, :], 0.0), axis=1, keepdims=True)
         match = column == expert
         member = jnp.where(match, 1.0, member)
-        weight = jnp.where(match, share, weight)
+        if weights_ref is not None:
+            share = weights_ref[k : k + 1, :]
+            share = jnp.sum(jnp.where(square, share, 0.0), axis=1, keepdims=True)
+            weight = jnp.where(match, share, weight)
     earlier = (
         lax.broadcasted_iota(jnp.int32, (rows, rows), 0)
         > lax.broadcasted_iota(jnp.int32, (rows, rows), 1)
@@ -157,22 +208,20 @@
     ranking = mm(jnp.where(earlier, 1.0, 0.0).astype(BF), member.astype(BF)).astype(jnp.int32)
     routed = jnp.where(ranking == kind, member, 0.0)
     own = jnp.where(row == ((slot >> 6) * 2 + kind - 2), 1.0, 0.0)
-    is_routed = kind < 2
-    place_ref[...] = jnp.where(is_routed, routed, own).astype(BF)
-    shares = jnp.where(is_routed, routed * weight, own)
-    high = shares.astype(BF)
-    high_ref[...] = high
-    low_ref[...] = (shares - high.astype(F32)).astype(BF)
-
-
-def middle_kernel(tp_ref, arrived_ref, layer_ref, place_ref, middle_ref, send_ref):
+    if weights_ref is not None:
+        routed = routed * weight
+    return jnp.where(kind < 2, routed, own)
+
+
+def middle_kernel(tp_ref, arrived_ref, layer_ref, ids_ref, middle_ref, send_ref):
+    place = routing(ids_ref, None, send_ref.shape[0]).astype(BF)
     total = arrived_ref[0].astype(F32)
     for t in range(1, arrived_ref.shape[0]):
         total = total + arrived_ref[t].astype(F32)
     start = pl.multiple_of(tp_ref[0] * LANES, LANES)
     middle = (layer_ref[:, pl.ds(start, LANES)].astype(F32) + total).astype(BF)
     middle_ref[...] = middle
-    send_ref[...] = tn(place_ref[...], middle).astype(BF)
+    send_ref[...] = tn(place, middle).astype(BF)
 
 
 def expert_kernel(
@@ -181,12 +230,20 @@
     gate_ref,
     up_ref,
     down_ref,
+    sgate_hbm,
+    sup_hbm,
+    sdown_hbm,
+    send_ref,
+    wide_ref,
     sgate_ref,
     sup_ref,
     sdown_ref,
-    send_ref,
-    wide_ref,
+    sems,
 ):
+    pairs = ((sgate_hbm, sgate_ref), (sup_hbm, sup_ref), (sdown_hbm, sdown_ref))
+    copies = [pltpu.make_async_copy(a, b, sems.at[i]) for i, (a, b) in enumerate(pairs)]
+    for copy in copies:
+        copy.start()
     groups = 16
     kinds = 4
     stride = arrived_ref.shape[0] // groups
@@ -207,6 +264,8 @@
     shared = rms_rows(jnp.concatenate([rows_of(2), rows_of(3)], axis=0), gain)
     hidden = (swish(mm(routed, gate_ref[0])) * mm(routed, up_ref[0])).astype(BF)
     served = mm(hidden, down_ref[0])
+    for copy in copies:
+        copy.wait()
     shidden = (swish(nt(shared, sgate_ref[...])) * nt(shared, sup_ref[...])).astype(BF)
     sserved = mm(shidden, sdown_ref[...])
     for s, block in enumerate((served, served, sserved, sserved)):
@@ -217,9 +276,12 @@
     send_ref[...] = wide_ref[...].astype(BF)
 
 
-def combine_kernel(arrived_ref, high_ref, low_ref, middle_ref, send_ref):
+def combine_kernel(arrived_ref, ids_ref, weights_ref, middle_ref, send_ref):
+    shares = routing(ids_ref, weights_ref, arrived_ref.shape[0])
+    high = shares.astype(BF)
+    low = (shares - high.astype(F32)).astype(BF)
     arrived = arrived_ref[...]
-    total = mm(high_ref[...], arrived) + mm(low_ref[...], arrived)
+    total = mm(high, arrived) + mm(low, arrived)
     out = (middle_ref[...].astype(F32) + total).astype(BF)
     for t in range(send_ref.shape[0]):
         send_ref[t] = out
@@ -227,6 +289,10 @@
 
 def exchange(x, axes):
     return lax.all_to_all(x, axes, split_axis=0, concat_axis=0, tiled=True)
+
+
+def far(x):
+    return pltpu.with_memory_space_constraint(x, pltpu.HBM)
 
 
 def call(kernel, outs, in_specs, scratch=(), limit=16 << 20):
@@ -263,6 +329,8 @@
 ):
     rows, width = layer_in.shape
     span = kv_cache.shape[2]
+    hd = query_weight.shape[1]
+    gates = forget_weight.shape[1]
     tp_count = lax.axis_size(TP)
     everyone = lax.axis_size(ALL)
     tp = lax.axis_index(TP).astype(jnp.int32).reshape(1)
@@ -272,14 +340,25 @@
     vmem = pl.BlockSpec(memory_space=pltpu.VMEM)
     hbm = pl.BlockSpec(memory_space=pltpu.HBM)
 
-    place, high, low = call(
-        route_kernel, [shape((rows, slots), BF)] * 3, in_specs=[vmem] * 2
-    )(route_ids.T, route_weights.T)
+    ids = route_ids.T
     part, new_kv = call(
         attention_kernel,
         [shape((tp_count, rows, LANES), BF), shape((rows, LANES), BF)],
-        in_specs=[smem] * 3 + [vmem] * 8 + [hbm],
-        scratch=[pltpu.VMEM((span, rows * LANES), BF), pltpu.SemaphoreType.DMA((rows,))],
+        in_specs=[hbm] * 2 + [smem] + [hbm] * 9,
+        scratch=[
+            VMEM((span, rows * LANES), BF),
+            pltpu.SMEM((rows,), jnp.int32),
+            pltpu.SMEM((gates,), F32),
+            VMEM((rows, width), BF),
+            VMEM((1, width), F32),
+            VMEM((2 * hd + gates, width), BF),
+            VMEM((2 * hd, width), BF),
+            VMEM((hd, width), BF),
+            VMEM((rows, 1, span), F32),
+            VMEM((span, LANES), F32),
+            pltpu.SemaphoreType.DMA((rows,)),
+            pltpu.SemaphoreType.DMA((11,)),
+        ],
         limit=60 * 1024 * 1024,
     )(
         lengths,
@@ -300,27 +379,29 @@
         middle_kernel,
         [shape((rows, LANES), BF), shape((slots, LANES), BF)],
         in_specs=[smem] + [vmem] * 3,
-    )(tp, arrived, layer_in, place)
+    )(tp, arrived, layer_in, ids)
     arrived = exchange(send.reshape(everyone, 4, LANES), ALL).reshape(slots, LANES)
     send = call(
         expert_kernel,
         shape((slots, LANES), BF),
-        in_specs=[vmem] * 8,
-        scratch=[pltpu.VMEM((slots, LANES), F32)],
+        in_specs=[vmem] * 5 + [hbm] * 3,
+        scratch=[VMEM((slots, LANES), F32)]
+        + [VMEM((shared_gate.shape[1], width), BF)] * 3
+        + [pltpu.SemaphoreType.DMA((3,))],
     )(
         arrived,
         ffn_gain.reshape(1, width),
         expert_gate,
         expert_up,
         expert_down,
-        shared_gate.T,
-        shared_up.T,
-        shared_down,
+        far(shared_gate.T),
+        far(shared_up.T),
+        far(shared_down),
     )
     arrived = exchange(send.reshape(everyone, 4, LANES), ALL).reshape(slots, LANES)
     send = call(
         combine_kernel, shape((tp_count, rows, LANES), BF), in_specs=[vmem] * 4
-    )(arrived, high, low, middle)
+    )(arrived, ids, route_weights.T, middle)
     out = exchange(send, TP)
     layer_out = out.transpose(1, 0, 2).reshape(rows, width)
     return (layer_out, new_kv.reshape(rows, 1, LANES))

time: 96.3 us -> 90.3 us (0.938)
  blocking collectives: 57.6 us -> 76.4 us
  starting transfers between devices: 9.98 us -> 0 us
  waiting for transfers between devices: 6.71 us -> 0 us
  local copies, waits for them, and re-layouts: 6.87 us -> 0.69 us
  Pallas kernels: 13.9 us -> 12.2 us
    all_to_all x3 -> x4, blocking collectives: 57.6 us -> 76.4 us  [exchange(): return lax.all_to_all(x, axes, split_axis=0, concat_axis=0, tiled=True)]
    all_to_all x1 -> x0, starting transfers between devices: 9.98 us -> none  [exchange(): return lax.all_to_all(x, axes, split_axis=0, concat_axis=0, tiled=True)]
    all_to_all x1 -> x0, waiting for transfers between devices: 6.71 us -> none  [exchange(): return lax.all_to_all(x, axes, split_axis=0, concat_axis=0, tiled=True)]
    unnamed x32 -> x14, local copies, waits for them, and re-layouts: 6.2 us -> 0.03 us
    pallas_call x1, Pallas kernels: 11.7 us -> 8.47 us  [body(): call(attention_kernel, [shape((tp_count, rows, LANES), BF), shape((rows,...]
    pallas_call x2 -> x1, Pallas kernels: 1.73 us -> 2.72 us  [body(): call(expert_kernel, shape((slots, LANES), BF), in_specs=[vmem] * 5 + [hbm...]
  transfers between devices with their start and end apart: 1 -> 0, of which waited for: 1 -> 0; matrix products, arithmetic and copies ran while one was open for 0% -> 0% of each run, Pallas kernels for 0% -> 0%
where the time goes in v3:
time: 90.3 us; the launch traced here: 90.1 us
  blocking collectives  76.4 us (85%)
  Pallas kernels  12.2 us (14%)
    all_to_all x4, blocking collectives, exchange(): return lax.all_to_all(x, axes, split_axis=0, concat_axis=0, tiled=True)  76.4 us
    pallas_call x1, Pallas kernels, body(): call(attention_kernel, [shape((tp_count, rows, LANES), BF), shape((rows,...  8.47 us
    pallas_call x1, Pallas kernels, body(): call(expert_kernel, shape((slots, LANES), BF), in_specs=[vmem] * 5 + [hbm...  2.72 us

profile of v3, /device:TPU:1, one launch (start us, length us, event | category | flops | bytes accessed | tf_op | source)
XLA Modules:
  0.0 90.1 jit_solution(1135797557298154092)
XLA Ops:
  0.6 0.0 copy-start.3
  0.6 0.0 copy-start.4
  0.7 0.0 copy-start.2
  0.7 0.0 copy-start.1
  0.7 0.0 copy-start
  0.7 0.0 copy-start.5
  0.7 0.0 copy-start.6
  0.7 8.5 %shard_map.203 = (bf16[16,32,128]{2,1,0:T(8,128)(2,1)}, bf16[32,128]{1,0:T(8,128)(2,1)}) custom-call(s32[32]{0:T(128)} %lengths_hbm.1, f32[16]{0:T(128)} %bias_hbm.1, s32[1]{0:T(128)} %bitcast.head_ref.tp_ref, bf16[32,2048]{1,0:T(8,128)(2,1)} %layer_ref.1, f32[1,2048]{1,0:T(1,128)} %bitcast.36, bf16[64,2048]{1,0:T(8,128)(2,1)} %bitcast.30, ...), custom_call_target="tpu_custom_call" | custom-call | tf_op jit(solution)/shard_map/pallas_call | solution.py:344
  9.2 18.9 %all_to_all.20.arrived_ref = bf16[16,32,128]{2,1,0:T(8,128)(2,1)S(1)} all-to-all(bf16[16,32,128]{2,1,0:T(8,128)(2,1)} %get-tuple-element.6), channel_id=1, replica_groups=mesh['y'=4,'x'=4,'z'=8,'c'=2] {'z','c'}, dimensions={0} | all-to-all | bytes 262144 | tf_op jit(solution)/shard_map/all_to_all | solution.py:291
  28.1 0.0 copy-done.3
  28.1 0.0 copy-done.4
  28.1 0.5 shard_map.204
  28.6 24.2 %all_to_all.21 = bf16[256,4,128]{2,1,0:T(4,128)(2,1)S(1)} all-to-all(bf16[256,4,128]{2,1,0:T(4,128)(2,1)S(1)} %bitcast.25), channel_id=1, replica_groups=mesh['y'=4,'x'=4,'z'=8,'c'=2] {'y','x','z','c'}, dimensions={0} | all-to-all | bytes 524288 | tf_op jit(solution)/shard_map/all_to_all | solution.py:291
  52.8 0.0 copy-done.2
  52.8 0.0 copy-done.1
  52.8 0.0 copy-done
  52.8 0.0 copy-done.5
  52.8 2.7 %shard_map.205 = bf16[1024,128]{1,0:T(8,128)(2,1)S(1)} custom-call(bf16[1024,128]{1,0:T(8,128)(2,1)S(1)} %bitcast.22, f32[1,2048]{1,0:T(1,128)S(1)} %bitcast.28, bf16[1,2048,256]{2,1,0:T(8,128)(2,1)S(1)} %copy-done, bf16[1,2048,256]{2,1,0:T(8,128)(2,1)S(1)} %copy-done.1, bf16[1,256,2048]{2,1,0:T(8,128)(2,1)S(1)} %copy-done.2, bf16[32,2048]{1,0:T(8,128)(2,1)} %bitcast.33, ...), custom_call_target="tpu_custom_call" | custom-call | tf_op jit(solution)/shard_map/pallas_call | solution.py:384
  55.6 21.2 %all_to_all.22 = bf16[256,4,128]{2,1,0:T(4,128)(2,1)S(1)} all-to-all(bf16[256,4,128]{2,1,0:T(4,128)(2,1)S(1)} %bitcast.23), channel_id=1, replica_groups=mesh['y'=4,'x'=4,'z'=8,'c'=2] {'y','x','z','c'}, dimensions={0} | all-to-all | bytes 524288 | tf_op jit(solution)/shard_map/all_to_all | solution.py:291
  76.8 0.0 copy-done.6
  76.8 0.5 shard_map.206
  77.3 12.1 %all_to_all.23 = bf16[16,32,128]{2,1,0:T(8,128)(2,1)S(1)} all-to-all(bf16[16,32,128]{2,1,0:T(8,128)(2,1)S(1)} %shard_map.206), channel_id=1, replica_groups=mesh['y'=4,'x'=4,'z'=8,'c'=2] {'z','c'}, dimensions={0} | all-to-all | bytes 262144 | tf_op jit(solution)/shard_map/all_to_all | solution.py:291
  89.4 0.7 copy_bitcast_fusion
Async XLA Ops:
  0.6 27.4 %copy-start.3 = (bf16[32,2048]{1,0:T(8,128)(2,1)S(1)}, bf16[32,2048]{1,0:T(8,128)(2,1)}, u32[]{:S(2)}) copy-start(bf16[32,2048]{1,0:T(8,128)(2,1)} %layer_ref.1) | copy-start | bytes 393220
  0.6 27.4 %copy-start.4 = (s32[32,6]{0,1:T(8,128)S(1)}, s32[32,6]{0,1:T(8,128)}, u32[]{:S(2)}) copy-start(s32[32,6]{0,1:T(8,128)} %param.32) | copy-start | bytes 2308
  0.7 52.2 %copy-start.2 = (bf16[1,256,2048]{2,1,0:T(8,128)(2,1)S(1)}, bf16[1,256,2048]{2,1,0:T(8,128)(2,1)}, u32[]{:S(2)}) copy-start(bf16[1,256,2048]{2,1,0:T(8,128)(2,1)} %down_ref.1) | copy-start | bytes 3145732
  0.7 52.2 %copy-start.1 = (bf16[1,2048,256]{2,1,0:T(8,128)(2,1)S(1)}, bf16[1,2048,256]{2,1,0:T(8,128)(2,1)}, u32[]{:S(2)}) copy-start(bf16[1,2048,256]{2,1,0:T(8,128)(2,1)} %up_ref.1) | copy-start | bytes 3145732
  0.7 52.2 %copy-start = (bf16[1,2048,256]{2,1,0:T(8,128)(2,1)S(1)}, bf16[1,2048,256]{2,1,0:T(8,128)(2,1)}, u32[]{:S(2)}) copy-start(bf16[1,2048,256]{2,1,0:T(8,128)(2,1)} %gate_ref.1) | copy-start | bytes 3145732
  0.7 52.1 %copy-start.5 = (f32[2048]{0:T(1024)S(1)}, f32[2048]{0:T(1024)}, u32[]{:S(2)}) copy-start(f32[2048]{0:T(1024)} %param.31) | copy-start | bytes 24580
  0.7 76.1 %copy-start.6 = (f32[32,6]{0,1:T(8,128)S(1)}, f32[32,6]{0,1:T(8,128)}, u32[]{:S(2)}) copy-start(f32[32,6]{0,1:T(8,128)} %param.33) | copy-start | bytes 2308

commit v4 on v3

--- a/solution.py
+++ b/solution.py
@@ -90,7 +90,7 @@
         fetch(s).start()
         return carry
 
-    for copy in small[:6] + small[9:]:
+    for copy in small:
         copy.start()
     lax.fori_loop(0, rows, start, 0)
 
@@ -101,8 +101,6 @@
     for s in range(rows):
         length = jnp.where(lane == s, lengths_ref[s], length)
 
-    for copy in small[6:9]:
-        copy.start()
     normed = rms_rows(layer_ref[...].astype(F32), gain_ref[...])
     padded = jnp.concatenate([normed, jnp.zeros((LANES - rows, width), BF)], axis=0)
     by_seq = nt(first_ref[...], padded)
@@ -127,6 +125,10 @@
     latest = jnp.sum(jnp.where(position == length - 1, cum, 0.0), axis=0, keepdims=True)
     shift = (latest + forget) - cum
 
+    for copy in small[6:9]:
+        copy.wait()
+    new_kv = nt(normed, second_ref[...]).astype(BF)
+    newkv_ref[...] = new_kv
     query = jnp.concatenate([query, jnp.zeros((LANES - hd, LANES), F32)], axis=0)
     lane_full = lax.broadcasted_iota(jnp.int32, (LANES, LANES), 1)
     score_ref[...] = shift
@@ -153,17 +155,13 @@
     probs = jnp.transpose(earlier * inverse)[:rows].astype(BF)
     own = (own * inverse).astype(BF).astype(F32)
 
-    for copy in small[6:9]:
-        copy.wait()
-    new_kv = nt(normed, second_ref[...]).astype(BF)
-    newkv_ref[...] = new_kv
     square_row = lax.broadcasted_iota(jnp.int32, (rows, LANES), 0)
     square_lane = lax.broadcasted_iota(jnp.int32, (rows, LANES), 1)
     own_column = jnp.sum(
         jnp.where(square_row == square_lane, own, 0.0), axis=1, keepdims=True
     )
     blended = own_column * new_kv.astype(F32)
-    step = 8
+    step = 16
 
     def value_step(i, total):
         for k in range(step):
@@ -230,20 +228,16 @@
     gate_ref,
     up_ref,
     down_ref,
-    sgate_hbm,
-    sup_hbm,
+    sgate_ref,
+    sup_ref,
     sdown_hbm,
     send_ref,
     wide_ref,
-    sgate_ref,
-    sup_ref,
     sdown_ref,
-    sems,
+    sem,
 ):
-    pairs = ((sgate_hbm, sgate_ref), (sup_hbm, sup_ref), (sdown_hbm, sdown_ref))
-    copies = [pltpu.make_async_copy(a, b, sems.at[i]) for i, (a, b) in enumerate(pairs)]
-    for copy in copies:
-        copy.start()
+    copy = pltpu.make_async_copy(sdown_hbm, sdown_ref, sem)
+    copy.start()
     groups = 16
     kinds = 4
     stride = arrived_ref.shape[0] // groups
@@ -264,9 +258,8 @@
     shared = rms_rows(jnp.concatenate([rows_of(2), rows_of(3)], axis=0), gain)
     hidden = (swish(mm(routed, gate_ref[0])) * mm(routed, up_ref[0])).astype(BF)
     served = mm(hidden, down_ref[0])
-    for copy in copies:
-        copy.wait()
     shidden = (swish(nt(shared, sgate_ref[...])) * nt(shared, sup_ref[...])).astype(BF)
+    copy.wait()
     sserved = mm(shidden, sdown_ref[...])
     for s, block in enumerate((served, served, sserved, sserved)):
         for t in range(tiles):
@@ -359,20 +352,20 @@
             pltpu.SemaphoreType.DMA((rows,)),
             pltpu.SemaphoreType.DMA((11,)),
         ],
-        limit=60 * 1024 * 1024,
+        limit=24 << 20,
     )(
-        lengths,
-        forget_bias,
+        far(lengths),
+        far(forget_bias),
         tp,
-        layer_in,
-        attn_gain.reshape(1, width),
-        query_weight.T,
-        key_weight.T,
-        value_weight.T,
-        forget_weight.T,
-        out_weight,
-        cum_gates,
-        kv_cache,
+        far(layer_in),
+        far(attn_gain.reshape(1, width)),
+        far(query_weight.T),
+        far(key_weight.T),
+        far(value_weight.T),
+        far(forget_weight.T),
+        far(out_weight),
+        far(cum_gates),
+        far(kv_cache),
     )
     arrived = exchange(part, TP)
     middle, send = call(
@@ -384,18 +377,20 @@
     send = call(
         expert_kernel,
         shape((slots, LANES), BF),
-        in_specs=[vmem] * 5 + [hbm] * 3,
-        scratch=[VMEM((slots, LANES), F32)]
-        + [VMEM((shared_gate.shape[1], width), BF)] * 3
-        + [pltpu.SemaphoreType.DMA((3,))],
+        in_specs=[vmem] * 7 + [hbm],
+        scratch=[
+            VMEM((slots, LANES), F32),
+            VMEM(shared_down.shape, BF),
+            pltpu.SemaphoreType.DMA,
+        ],
     )(
         arrived,
         ffn_gain.reshape(1, width),
         expert_gate,
         expert_up,
         expert_down,
-        far(shared_gate.T),
-        far(shared_up.T),
+        shared_gate.T,
+        shared_up.T,
         far(shared_down),
     )
     arrived = exchange(send.reshape(everyone, 4, LANES), ALL).reshape(slots, LANES)

time: 90.3 us -> 89.2 us (0.988)
  Pallas kernels: 12.2 us -> 11.2 us
where the time goes in v4:
time: 89.2 us; the launch traced here: 88.9 us
  blocking collectives  76.2 us (85%)
  Pallas kernels  11.2 us (13%)
    all_to_all x4, blocking collectives, exchange(): return lax.all_to_all(x, axes, split_axis=0, concat_axis=0, tiled=True)  76.2 us
    pallas_call x1, Pallas kernels, body(): call(attention_kernel, [shape((tp_count, rows, LANES), BF), shape((rows,...  7.83 us
    pallas_call x1, Pallas kernels, body(): call(expert_kernel, shape((slots, LANES), BF), in_specs=[vmem] * 7 + [hbm...  2.42 us

profile of v4, /device:TPU:1, one launch (start us, length us, event | category | flops | bytes accessed | tf_op | source)
XLA Modules:
  0.0 88.9 jit_solution(8895050088496724549)
XLA Ops:
  0.6 0.0 copy-start.3
  0.6 0.0 copy-start.6
  0.7 0.0 copy-start.2
  0.7 0.0 copy-start.1
  0.7 0.0 copy-start
  0.7 0.0 copy-start.5
  0.7 0.0 copy-start.4
  0.7 0.0 copy-start.7
  0.7 0.0 copy-start.8
  0.7 7.8 %shard_map.203 = (bf16[16,32,128]{2,1,0:T(8,128)(2,1)S(1)}, bf16[32,128]{1,0:T(8,128)(2,1)}) custom-call(s32[32]{0:T(128)} %lengths_hbm.1, f32[16]{0:T(128)} %bias_hbm.1, s32[1]{0:T(128)} %bitcast.head_ref.tp_ref, bf16[32,2048]{1,0:T(8,128)(2,1)} %layer_ref.1, f32[1,2048]{1,0:T(1,128)} %bitcast.36, bf16[64,2048]{1,0:T(8,128)(2,1)} %bitcast.32, ...), custom_call_target="tpu_custom_call" | custom-call | tf_op jit(solution)/shard_map/pallas_call | solution.py:337
  8.6 18.7 %all_to_all.20.arrived_ref = bf16[16,32,128]{2,1,0:T(8,128)(2,1)S(1)} all-to-all(bf16[16,32,128]{2,1,0:T(8,128)(2,1)S(1)} %get-tuple-element.6), channel_id=1, replica_groups=mesh['y'=4,'x'=4,'z'=8,'c'=2] {'z','c'}, dimensions={0} | all-to-all | bytes 262144 | tf_op jit(solution)/shard_map/all_to_all | solution.py:284
  27.2 0.0 copy-done.3
  27.2 0.0 copy-done.6
  27.2 0.5 shard_map.204
  27.7 24.2 %all_to_all.21 = bf16[256,4,128]{2,1,0:T(4,128)(2,1)S(1)} all-to-all(bf16[256,4,128]{2,1,0:T(4,128)(2,1)S(1)} %bitcast.25), channel_id=1, replica_groups=mesh['y'=4,'x'=4,'z'=8,'c'=2] {'y','x','z','c'}, dimensions={0} | all-to-all | bytes 524288 | tf_op jit(solution)/shard_map/all_to_all | solution.py:284
  52.0 0.0 copy-done
  52.0 0.0 copy-done.5
  52.0 0.0 copy-done.4
  52.0 0.0 copy-done.7
  52.0 2.4 %shard_map.205 = bf16[1024,128]{1,0:T(8,128)(2,1)S(1)} custom-call(bf16[1024,128]{1,0:T(8,128)(2,1)S(1)} %bitcast.22, f32[1,2048]{1,0:T(1,128)S(1)} %bitcast.30, bf16[1,2048,256]{2,1,0:T(8,128)(2,1)S(1)} %copy-done, bf16[1,2048,256]{2,1,0:T(8,128)(2,1)S(1)} %copy-done.1, bf16[1,256,2048]{2,1,0:T(8,128)(2,1)S(1)} %copy-done.2, bf16[32,2048]{1,0:T(8,128)(2,1)S(1)} %bitcast.26, ...), custom_call_target="tpu_custom_call" | custom-call | tf_op jit(solution)/shard_map/pallas_call | solution.py:377
  54.5 21.2 %all_to_all.22 = bf16[256,4,128]{2,1,0:T(4,128)(2,1)S(1)} all-to-all(bf16[256,4,128]{2,1,0:T(4,128)(2,1)S(1)} %bitcast.23), channel_id=1, replica_groups=mesh['y'=4,'x'=4,'z'=8,'c'=2] {'y','x','z','c'}, dimensions={0} | all-to-all | bytes 524288 | tf_op jit(solution)/shard_map/all_to_all | solution.py:284
  75.7 0.5 shard_map.206
  76.2 12.1 %all_to_all.23 = bf16[16,32,128]{2,1,0:T(8,128)(2,1)S(1)} all-to-all(bf16[16,32,128]{2,1,0:T(8,128)(2,1)S(1)} %shard_map.206), channel_id=1, replica_groups=mesh['y'=4,'x'=4,'z'=8,'c'=2] {'z','c'}, dimensions={0} | all-to-all | bytes 262144 | tf_op jit(solution)/shard_map/all_to_all | solution.py:284
  88.3 0.7 copy_bitcast_fusion
  (3 shorter events, 0.0 us)
Async XLA Ops:
  0.6 26.6 %copy-start.3 = (bf16[32,2048]{1,0:T(8,128)(2,1)S(1)}, bf16[32,2048]{1,0:T(8,128)(2,1)}, u32[]{:S(2)}) copy-start(bf16[32,2048]{1,0:T(8,128)(2,1)} %layer_ref.1) | copy-start | bytes 393220
  0.6 26.6 %copy-start.6 = (s32[32,6]{0,1:T(8,128)S(1)}, s32[32,6]{0,1:T(8,128)}, u32[]{:S(2)}) copy-start(s32[32,6]{0,1:T(8,128)} %param.32) | copy-start | bytes 2308
  0.7 51.3 %copy-start.2 = (bf16[1,256,2048]{2,1,0:T(8,128)(2,1)S(1)}, bf16[1,256,2048]{2,1,0:T(8,128)(2,1)}, u32[]{:S(2)}) copy-start(bf16[1,256,2048]{2,1,0:T(8,128)(2,1)} %down_ref.1) | copy-start | bytes 3145732
  0.7 51.3 %copy-start.1 = (bf16[1,2048,256]{2,1,0:T(8,128)(2,1)S(1)}, bf16[1,2048,256]{2,1,0:T(8,128)(2,1)}, u32[]{:S(2)}) copy-start(bf16[1,2048,256]{2,1,0:T(8,128)(2,1)} %up_ref.1) | copy-start | bytes 3145732
  0.7 51.3 %copy-start = (bf16[1,2048,256]{2,1,0:T(8,128)(2,1)S(1)}, bf16[1,2048,256]{2,1,0:T(8,128)(2,1)}, u32[]{:S(2)}) copy-start(bf16[1,2048,256]{2,1,0:T(8,128)(2,1)} %gate_ref.1) | copy-start | bytes 3145732
  0.7 51.3 %copy-start.5 = (bf16[2048,32]{0,1:T(8,128)(2,1)S(1)}, bf16[2048,32]{0,1:T(8,128)(2,1)}, u32[]{:S(2)}) copy-start(bf16[2048,32]{0,1:T(8,128)(2,1)} %param.35) | copy-start | bytes 393220
  0.7 51.3 %copy-start.4 = (bf16[2048,32]{0,1:T(8,128)(2,1)S(1)}, bf16[2048,32]{0,1:T(8,128)(2,1)}, u32[]{:S(2)}) copy-start(bf16[2048,32]{0,1:T(8,128)(2,1)} %param.34) | copy-start | bytes 393220
  0.7 51.3 %copy-start.7 = (f32[2048]{0:T(1024)S(1)}, f32[2048]{0:T(1024)}, u32[]{:S(2)}) copy-start(f32[2048]{0:T(1024)} %param.31) | copy-start | bytes 24580
  0.7 75.0 %copy-start.8 = (f32[32,6]{0,1:T(8,128)S(1)}, f32[32,6]{0,1:T(8,128)}, u32[]{:S(2)}) copy-start(f32[32,6]{0,1:T(8,128)} %param.33) | copy-start | bytes 2308

commit v5 on v4

--- a/solution.py
+++ b/solution.py
@@ -15,6 +15,8 @@
 EP = ("y", "x")
 TP = ("z", "c")
 ALL = ("y", "x", "z", "c")
+CHIPS = ("y", "x", "z")
+SWAP = ((0, 1), (1, 0))
 
 
 def nt(a, b):
@@ -186,7 +188,7 @@
     )
     slot = lax.broadcasted_iota(jnp.int32, (rows, many), 1)
     row = lax.broadcasted_iota(jnp.int32, (rows, many), 0)
-    expert = slot >> 3
+    expert = slot >> 2
     kind = slot & 3
     weight = jnp.zeros((rows, many), F32)
     member = jnp.zeros((rows, many), F32)
@@ -205,7 +207,7 @@
     )
     ranking = mm(jnp.where(earlier, 1.0, 0.0).astype(BF), member.astype(BF)).astype(jnp.int32)
     routed = jnp.where(ranking == kind, member, 0.0)
-    own = jnp.where(row == ((slot >> 6) * 2 + kind - 2), 1.0, 0.0)
+    own = jnp.where(row == ((slot >> 5) * 2 + kind - 2), 1.0, 0.0)
     if weights_ref is not None:
         routed = routed * weight
     return jnp.where(kind < 2, routed, own)
@@ -223,7 +225,9 @@
 
 
 def expert_kernel(
-    arrived_ref,
+    core_ref,
+    mine_ref,
+    theirs_ref,
     gain_ref,
     gate_ref,
     up_ref,
@@ -231,8 +235,10 @@
     sgate_ref,
     sup_ref,
     sdown_hbm,
-    send_ref,
-    wide_ref,
+    keep_ref,
+    give_ref,
+    even_ref,
+    odd_ref,
     sdown_ref,
     sem,
 ):
@@ -240,13 +246,21 @@
     copy.start()
     groups = 16
     kinds = 4
-    stride = arrived_ref.shape[0] // groups
+    stride = mine_ref.shape[0] // groups
     tiles = stride // kinds
-    wide_ref[...] = arrived_ref[...].astype(F32)
+    first = core_ref[0] == 0
+    mine = mine_ref[...].astype(F32)
+    theirs = theirs_ref[...].astype(F32)
+    even_ref[...] = jnp.where(first, mine, theirs)
+    odd_ref[...] = jnp.where(first, theirs, mine)
+    sides = (even_ref, odd_ref)
 
     def rows_of(s):
         return jnp.concatenate(
-            [wide_ref[pl.ds(t * kinds + s, groups, stride=stride), :] for t in range(tiles)],
+            [
+                sides[t % 2][pl.ds((t // 2) * kinds + s, groups, stride=stride), :]
+                for t in range(2 * tiles)
+            ],
             axis=1,
         )
 
@@ -262,11 +276,14 @@
     copy.wait()
     sserved = mm(shidden, sdown_ref[...])
     for s, block in enumerate((served, served, sserved, sserved)):
-        for t in range(tiles):
-            wide_ref[pl.ds(t * kinds + s, groups, stride=stride), :] = block[
+        for t in range(2 * tiles):
+            sides[t % 2][pl.ds((t // 2) * kinds + s, groups, stride=stride), :] = block[
                 (s % 2) * groups : (s % 2 + 1) * groups, t * LANES : (t + 1) * LANES
             ]
-    send_ref[...] = wide_ref[...].astype(BF)
+    even = even_ref[...]
+    odd = odd_ref[...]
+    keep_ref[...] = jnp.where(first, even, odd)
+    give_ref[...] = jnp.where(first, odd, even).astype(BF)
 
 
 def combine_kernel(arrived_ref, ids_ref, weights_ref, middle_ref, send_ref):
@@ -325,9 +342,10 @@
     hd = query_weight.shape[1]
     gates = forget_weight.shape[1]
     tp_count = lax.axis_size(TP)
-    everyone = lax.axis_size(ALL)
+    chips = lax.axis_size(CHIPS)
+    core = lax.axis_index("c").astype(jnp.int32).reshape(1)
     tp = lax.axis_index(TP).astype(jnp.int32).reshape(1)
-    slots = everyone * 4
+    slots = chips * 4
     shape = jax.ShapeDtypeStruct
     smem = pl.BlockSpec(memory_space=pltpu.SMEM)
     vmem = pl.BlockSpec(memory_space=pltpu.VMEM)
@@ -373,18 +391,22 @@
         [shape((rows, LANES), BF), shape((slots, LANES), BF)],
         in_specs=[smem] + [vmem] * 3,
     )(tp, arrived, layer_in, ids)
-    arrived = exchange(send.reshape(everyone, 4, LANES), ALL).reshape(slots, LANES)
-    send = call(
+    mine = exchange(send.reshape(chips, 4, LANES), CHIPS).reshape(slots, LANES)
+    theirs = lax.ppermute(mine, "c", SWAP)
+    keep, give = call(
         expert_kernel,
-        shape((slots, LANES), BF),
-        in_specs=[vmem] * 7 + [hbm],
+        [shape((slots, LANES), F32), shape((slots, LANES), BF)],
+        in_specs=[smem] + [vmem] * 8 + [hbm],
         scratch=[
+            VMEM((slots, LANES), F32),
             VMEM((slots, LANES), F32),
             VMEM(shared_down.shape, BF),
             pltpu.SemaphoreType.DMA,
         ],
     )(
-        arrived,
+        core,
+        mine,
+        theirs,
         ffn_gain.reshape(1, width),
         expert_gate,
         expert_up,
@@ -393,7 +415,8 @@
         shared_up.T,
         far(shared_down),
     )
-    arrived = exchange(send.reshape(everyone, 4, LANES), ALL).reshape(slots, LANES)
+    send = (keep + lax.ppermute(give, "c", SWAP).astype(F32)).astype(BF)
+    arrived = exchange(send.reshape(chips, 4, LANES), CHIPS).reshape(slots, LANES)
     send = call(
         combine_kernel, shape((tp_count, rows, LANES), BF), in_specs=[vmem] * 4
     )(arrived, ids, route_weights.T, middle)

time: 89.2 us -> 86.8 us (0.973)
  blocking collectives: 76.2 us -> 69.8 us
  starting transfers between devices: 0 us -> 2.18 us
  waiting for transfers between devices: 0 us -> 1.97 us
    all_to_all x4, blocking collectives: 76.2 us -> 69.8 us  [exchange(): return lax.all_to_all(x, axes, split_axis=0, concat_axis=0, tiled=True)]
    ppermute x0 -> x2, starting transfers between devices: none -> 2.18 us  [the longest x1 1.72 us: body(): theirs = lax.ppermute(mine, 'c', SWAP)]
    ppermute x0 -> x2, waiting for transfers between devices: none -> 1.97 us  [the longest x1 0.99 us: body(): theirs = lax.ppermute(mine, 'c', SWAP)]
  transfers between devices with their start and end apart: 0 -> 2, of which waited for: 0 -> 2; matrix products, arithmetic and copies ran while one was open for 0% -> 0% of each run, Pallas kernels for 0% -> 0%
where the time goes in v5:
time: 86.8 us; the launch traced here: 86.6 us
  blocking collectives  69.8 us (80%)
  Pallas kernels  11.2 us (13%)
  starting transfers between devices  2.18 us (3%)
  waiting for transfers between devices  1.97 us (2%)
    all_to_all x4, blocking collectives, exchange(): return lax.all_to_all(x, axes, split_axis=0, concat_axis=0, tiled=True)  69.8 us
    pallas_call x1, Pallas kernels, body(): call(attention_kernel, [shape((tp_count, rows, LANES), BF), shape((rows,...  7.82 us
    pallas_call x1, Pallas kernels, body(): call(expert_kernel, [shape((slots, LANES), F32), shape((slots, LANES), BF...  2.48 us
  transfers between devices with their start and end apart: 2, of which 2 were waited for; matrix products, arithmetic and copies ran while one was open for 0% of the time, Pallas kernels for 0%

profile of v5, /device:TPU:1, one launch (start us, length us, event | category | flops | bytes accessed | tf_op | source)
XLA Modules:
  0.0 86.6 jit_solution(380362462767267495)
XLA Ops:
  0.6 0.0 copy-start.3
  0.6 0.0 copy-start.6
  0.7 0.0 copy-start.2
  0.7 0.0 copy-start.1
  0.7 0.0 copy-start
  0.7 0.0 copy-start.5
  0.7 0.0 copy-start.4
  0.7 0.0 copy-start.7
  0.7 0.0 copy-start.8
  0.7 7.8 %shard_map.203 = (bf16[16,32,128]{2,1,0:T(8,128)(2,1)S(1)}, bf16[32,128]{1,0:T(8,128)(2,1)}) custom-call(s32[32]{0:T(128)} %lengths_hbm.1, f32[16]{0:T(128)} %bias_hbm.1, s32[1]{0:T(128)} %bitcast.1.head_ref.tp_ref, bf16[32,2048]{1,0:T(8,128)(2,1)} %layer_ref.1, f32[1,2048]{1,0:T(1,128)} %bitcast.38, bf16[64,2048]{1,0:T(8,128)(2,1)} %bitcast.34, ...), custom_call_target="tpu_custom_call" | custom-call | tf_op jit(solution)/shard_map/pallas_call | solution.py:355
  8.6 18.7 %all_to_all.20.arrived_ref = bf16[16,32,128]{2,1,0:T(8,128)(2,1)S(1)} all-to-all(bf16[16,32,128]{2,1,0:T(8,128)(2,1)S(1)} %get-tuple-element.8), channel_id=1, replica_groups=mesh['y'=4,'x'=4,'z'=8,'c'=2] {'z','c'}, dimensions={0} | all-to-all | bytes 262144 | tf_op jit(solution)/shard_map/all_to_all | solution.py:301
  27.2 0.0 copy-done.3
  27.2 0.4 shard_map.204
  27.7 20.8 %all_to_all.21 = bf16[128,4,128]{2,1,0:T(4,128)(2,1)S(1)} all-to-all(bf16[128,4,128]{2,1,0:T(4,128)(2,1)S(1)} %bitcast.28), channel_id=1, replica_groups=mesh['y'=4,'x'=4,'z'=8,'c'=2] {'y','x','z'}, dimensions={0} | all-to-all | bytes 262144 | tf_op jit(solution)/shard_map/all_to_all | solution.py:301
  48.5 1.7 %collective-permute-start = (bf16[512,128]{1,0:T(8,128)(2,1)S(1)}, bf16[512,128]{1,0:T(8,128)(2,1)S(1)}, u32[]{:S(2)}, u32[]{:S(2)}) collective-permute-start(bf16[512,128]{1,0:T(8,128)(2,1)S(1)} %bitcast.23), channel_id=1, source_target_pairs={{0,1},{1,0},{2,3},{3,2},{4,5},{5,4},{6,7},{7,6},{8,9},{9,8},{10,11... | collective-permute-start | bytes 393224 | tf_op jit(solution)/shard_map/ppermute | solution.py:395
  50.2 1.0 %collective-permute-done.theirs_ref = bf16[512,128]{1,0:T(8,128)(2,1)S(1)} collective-permute-done((bf16[512,128]{1,0:T(8,128)(2,1)S(1)}, bf16[512,128]{1,0:T(8,128)(2,1)S(1)}, u32[]{:S(2)}, u32[]{:S(2)}) %collective-permute-start) | collective-permute-done | bytes 131104 | tf_op jit(solution)/shard_map/ppermute | solution.py:395
  51.2 0.0 copy-done
  51.2 2.5 %shard_map.205 = (f32[512,128]{1,0:T(8,128)S(1)}, bf16[512,128]{1,0:T(8,128)(2,1)S(1)}) custom-call(s32[1]{0:T(128)} %bitcast.core_ref, bf16[512,128]{1,0:T(8,128)(2,1)S(1)} %bitcast.24, bf16[512,128]{1,0:T(8,128)(2,1)S(1)} %collective-permute-done.theirs_ref, f32[1,2048]{1,0:T(1,128)S(1)} %bitcast.31, bf16[1,2048,256]{2,1,0:T(8,128)(2,1)S(1)} %copy-done, ...), custom_call_target="tpu_custom_call" | custom-call | tf_op jit(solution)/shard_map/pallas_call | solution.py:396
  53.7 0.5 collective-permute-start.1
  54.2 1.0 %collective-permute-done.1 = bf16[512,128]{1,0:T(8,128)(2,1)S(1)} collective-permute-done((bf16[512,128]{1,0:T(8,128)(2,1)S(1)}, bf16[512,128]{1,0:T(8,128)(2,1)S(1)}, u32[]{:S(2)}, u32[]{:S(2)}) %collective-permute-start.1) | collective-permute-done | bytes 131104 | tf_op jit(solution)/shard_map/ppermute | solution.py:418
  55.2 17.2 %all_to_all.22 = bf16[128,4,128]{2,1,0:T(4,128)(2,1)S(1)} all-to-all(bf16[128,4,128]{2,1,0:T(4,128)(2,1)S(1)} %bitcast.33), channel_id=1, replica_groups=mesh['y'=4,'x'=4,'z'=8,'c'=2] {'y','x','z'}, dimensions={0} | all-to-all | bytes 262144 | tf_op jit(solution)/shard_map/all_to_all | solution.py:301
  72.4 0.4 shard_map.206
  72.8 13.1 %all_to_all.23 = bf16[16,32,128]{2,1,0:T(8,128)(2,1)S(1)} all-to-all(bf16[16,32,128]{2,1,0:T(8,128)(2,1)S(1)} %shard_map.206), channel_id=1, replica_groups=mesh['y'=4,'x'=4,'z'=8,'c'=2] {'z','c'}, dimensions={0} | all-to-all | bytes 262144 | tf_op jit(solution)/shard_map/all_to_all | solution.py:301
  85.9 0.7 copy_bitcast_fusion
  (8 shorter events, 0.0 us)
Async XLA Ops:
  0.6 26.6 %copy-start.3 = (bf16[32,2048]{1,0:T(8,128)(2,1)S(1)}, bf16[32,2048]{1,0:T(8,128)(2,1)}, u32[]{:S(2)}) copy-start(bf16[32,2048]{1,0:T(8,128)(2,1)} %layer_ref.1) | copy-start | bytes 393220
  0.6 26.6 %copy-start.6 = (s32[32,6]{0,1:T(8,128)S(1)}, s32[32,6]{0,1:T(8,128)}, u32[]{:S(2)}) copy-start(s32[32,6]{0,1:T(8,128)} %param.32) | copy-start | bytes 2308
  0.7 50.5 %copy-start.2 = (bf16[1,256,2048]{2,1,0:T(8,128)(2,1)S(1)}, bf16[1,256,2048]{2,1,0:T(8,128)(2,1)}, u32[]{:S(2)}) copy-start(bf16[1,256,2048]{2,1,0:T(8,128)(2,1)} %down_ref.1) | copy-start | bytes 3145732
  0.7 50.5 %copy-start.1 = (bf16[1,2048,256]{2,1,0:T(8,128)(2,1)S(1)}, bf16[1,2048,256]{2,1,0:T(8,128)(2,1)}, u32[]{:S(2)}) copy-start(bf16[1,2048,256]{2,1,0:T(8,128)(2,1)} %up_ref.1) | copy-start | bytes 3145732
  0.7 50.5 %copy-start = (bf16[1,2048,256]{2,1,0:T(8,128)(2,1)S(1)}, bf16[1,2048,256]{2,1,0:T(8,128)(2,1)}, u32[]{:S(2)}) copy-start(bf16[1,2048,256]{2,1,0:T(8,128)(2,1)} %gate_ref.1) | copy-start | bytes 3145732
  0.7 50.5 %copy-start.5 = (bf16[2048,32]{0,1:T(8,128)(2,1)S(1)}, bf16[2048,32]{0,1:T(8,128)(2,1)}, u32[]{:S(2)}) copy-start(bf16[2048,32]{0,1:T(8,128)(2,1)} %param.35) | copy-start | bytes 393220
  0.7 50.5 %copy-start.4 = (bf16[2048,32]{0,1:T(8,128)(2,1)S(1)}, bf16[2048,32]{0,1:T(8,128)(2,1)}, u32[]{:S(2)}) copy-start(bf16[2048,32]{0,1:T(8,128)(2,1)} %param.34) | copy-start | bytes 393220
  0.7 50.5 %copy-start.7 = (f32[2048]{0:T(1024)S(1)}, f32[2048]{0:T(1024)}, u32[]{:S(2)}) copy-start(f32[2048]{0:T(1024)} %param.31) | copy-start | bytes 24580
  0.7 71.7 %copy-start.8 = (f32[32,6]{0,1:T(8,128)S(1)}, f32[32,6]{0,1:T(8,128)}, u32[]{:S(2)}) copy-start(f32[32,6]{0,1:T(8,128)} %param.33) | copy-start | bytes 2308
  48.5 2.7 %collective-permute-start = (bf16[512,128]{1,0:T(8,128)(2,1)S(1)}, bf16[512,128]{1,0:T(8,128)(2,1)S(1)}, u32[]{:S(2)}, u32[]{:S(2)}) collective-permute-start(bf16[512,128]{1,0:T(8,128)(2,1)S(1)} %bitcast.23), channel_id=1, source_target_pairs={{0,1},{1,0},{2,3},{3,2},{4,5},{5,4},{6,7},{7,6},{8,9},{9,8},{10,11... | collective-permute-start | bytes 393224 | tf_op jit(solution)/shard_map/ppermute | solution.py:395
  53.7 1.4 %collective-permute-start.1 = (bf16[512,128]{1,0:T(8,128)(2,1)S(1)}, bf16[512,128]{1,0:T(8,128)(2,1)S(1)}, u32[]{:S(2)}, u32[]{:S(2)}) collective-permute-start(bf16[512,128]{1,0:T(8,128)(2,1)S(1)} %get-tuple-element.11), channel_id=1, source_target_pairs={{0,1},{1,0},{2,3},{3,2},{4,5},{5,4},{6,7},{7,6},{8,9},{9,8},{10,11... | collective-permute-start | bytes 393224 | tf_op jit(solution)/shard_map/ppermute | solution.py:418

commit v6 on v5

--- a/solution.py
+++ b/solution.py
@@ -75,8 +75,7 @@
         (wk_hbm, first_ref.at[hd : 2 * hd]),
         (wf_hbm, first_ref.at[2 * hd :]),
         (cum_hbm, cum_ref),
-        (wk_hbm, second_ref.at[:hd]),
-        (wv_hbm, second_ref.at[hd:]),
+        (wv_hbm, second_ref),
         (wo_hbm, wo_ref),
         (lengths_hbm, lengths_ref),
         (bias_hbm, bias_ref),
@@ -96,7 +95,7 @@
         copy.start()
     lax.fori_loop(0, rows, start, 0)
 
-    for copy in small[:5] + small[9:]:
+    for copy in small[:5] + small[8:]:
         copy.wait()
     lane = lax.broadcasted_iota(jnp.int32, (1, LANES), 1)
     length = jnp.zeros((1, LANES), jnp.int32)
@@ -127,9 +126,10 @@
     latest = jnp.sum(jnp.where(position == length - 1, cum, 0.0), axis=0, keepdims=True)
     shift = (latest + forget) - cum
 
-    for copy in small[6:9]:
+    for copy in small[6:8]:
         copy.wait()
-    new_kv = nt(normed, second_ref[...]).astype(BF)
+    new_kv = nt(normed, jnp.concatenate([first_ref[hd : 2 * hd], second_ref[...]], axis=0))
+    new_kv = new_kv.astype(BF)
     newkv_ref[...] = new_kv
     query = jnp.concatenate([query, jnp.zeros((LANES - hd, LANES), F32)], axis=0)
     lane_full = lax.broadcasted_iota(jnp.int32, (LANES, LANES), 1)
@@ -201,12 +201,11 @@
             share = weights_ref[k : k + 1, :]
             share = jnp.sum(jnp.where(square, share, 0.0), axis=1, keepdims=True)
             weight = jnp.where(match, share, weight)
-    earlier = (
-        lax.broadcasted_iota(jnp.int32, (rows, rows), 0)
-        > lax.broadcasted_iota(jnp.int32, (rows, rows), 1)
-    )
-    ranking = mm(jnp.where(earlier, 1.0, 0.0).astype(BF), member.astype(BF)).astype(jnp.int32)
-    routed = jnp.where(ranking == kind, member, 0.0)
+    named = member > 0.0
+    lowest = jnp.min(jnp.where(named, row, rows), axis=0, keepdims=True)
+    highest = jnp.max(jnp.where(named, row, -1), axis=0, keepdims=True)
+    wanted = jnp.where(kind == 0, lowest, jnp.where(highest == lowest, -1, highest))
+    routed = jnp.where(row == wanted, member, 0.0)
     own = jnp.where(row == ((slot >> 5) * 2 + kind - 2), 1.0, 0.0)
     if weights_ref is not None:
         routed = routed * weight
@@ -234,16 +233,12 @@
     down_ref,
     sgate_ref,
     sup_ref,
-    sdown_hbm,
+    sdown_ref,
     keep_ref,
     give_ref,
     even_ref,
     odd_ref,
-    sdown_ref,
-    sem,
 ):
-    copy = pltpu.make_async_copy(sdown_hbm, sdown_ref, sem)
-    copy.start()
     groups = 16
     kinds = 4
     stride = mine_ref.shape[0] // groups
@@ -273,7 +268,6 @@
     hidden = (swish(mm(routed, gate_ref[0])) * mm(routed, up_ref[0])).astype(BF)
     served = mm(hidden, down_ref[0])
     shidden = (swish(nt(shared, sgate_ref[...])) * nt(shared, sup_ref[...])).astype(BF)
-    copy.wait()
     sserved = mm(shidden, sdown_ref[...])
     for s, block in enumerate((served, served, sserved, sserved)):
         for t in range(2 * tiles):
@@ -363,12 +357,12 @@
             VMEM((rows, width), BF),
             VMEM((1, width), F32),
             VMEM((2 * hd + gates, width), BF),
-            VMEM((2 * hd, width), BF),
+            VMEM((hd, width), BF),
             VMEM((hd, width), BF),
             VMEM((rows, 1, span), F32),
             VMEM((span, LANES), F32),
             pltpu.SemaphoreType.DMA((rows,)),
-            pltpu.SemaphoreType.DMA((11,)),
+            pltpu.SemaphoreType.DMA((10,)),
         ],
         limit=24 << 20,
     )(
@@ -396,13 +390,8 @@
     keep, give = call(
         expert_kernel,
         [shape((slots, LANES), F32), shape((slots, LANES), BF)],
-        in_specs=[smem] + [vmem] * 8 + [hbm],
-        scratch=[
-            VMEM((slots, LANES), F32),
-            VMEM((slots, LANES), F32),
-            VMEM(shared_down.shape, BF),
-            pltpu.SemaphoreType.DMA,
-        ],
+        in_specs=[smem] + [vmem] * 9,
+        scratch=[VMEM((slots, LANES), F32)] * 2,
     )(
         core,
         mine,
@@ -413,7 +402,7 @@
         expert_down,
         shared_gate.T,
         shared_up.T,
-        far(shared_down),
+        shared_down,
     )
     send = (keep + lax.ppermute(give, "c", SWAP).astype(F32)).astype(BF)
     arrived = exchange(send.reshape(chips, 4, LANES), CHIPS).reshape(slots, LANES)

time: 86.8 us -> 85.7 us (0.987)
  Pallas kernels: 11.2 us -> 10 us
    pallas_call x1, Pallas kernels: 2.48 us -> 1.51 us  [body(): call(expert_kernel, [shape((slots, LANES), F32), shape((slots, LANES), BF...]
where the time goes in v6:
time: 85.7 us; the launch traced here: 85.5 us
  blocking collectives  69.8 us (81%)
  Pallas kernels  10 us (12%)
  starting transfers between devices  2.18 us (3%)
  waiting for transfers between devices  1.97 us (2%)
    all_to_all x4, blocking collectives, exchange(): return lax.all_to_all(x, axes, split_axis=0, concat_axis=0, tiled=True)  69.8 us
    pallas_call x1, Pallas kernels, body(): call(attention_kernel, [shape((tp_count, rows, LANES), BF), shape((rows,...  7.84 us
    ppermute x1, starting transfers between devices, body(): theirs = lax.ppermute(mine, 'c', SWAP)  1.72 us
  transfers between devices with their start and end apart: 2, of which 2 were waited for; matrix products, arithmetic and copies ran while one was open for 0% of the time, Pallas kernels for 0%

profile of v6, /device:TPU:1, one launch (start us, length us, event | category | flops | bytes accessed | tf_op | source)
XLA Modules:
  0.0 85.5 jit_solution(1920435735177612889)
XLA Ops:
  0.6 0.0 copy-start.3
  0.6 0.0 copy-start.7
  0.7 0.0 copy-start.2
  0.7 0.0 copy-start.1
  0.7 0.0 copy-start
  0.7 0.0 copy-start.5
  0.7 0.0 copy-start.4
  0.7 0.0 copy-start.8
  0.7 0.0 copy-start.9
  0.7 7.8 %shard_map.203 = (bf16[16,32,128]{2,1,0:T(8,128)(2,1)S(1)}, bf16[32,128]{1,0:T(8,128)(2,1)}) custom-call(s32[32]{0:T(128)} %lengths_hbm.1, f32[16]{0:T(128)} %bias_hbm.1, s32[1]{0:T(128)} %bitcast.1.head_ref.tp_ref, bf16[32,2048]{1,0:T(8,128)(2,1)} %layer_ref.1, f32[1,2048]{1,0:T(1,128)} %bitcast.38, bf16[64,2048]{1,0:T(8,128)(2,1)} %bitcast.34, ...), custom_call_target="tpu_custom_call" | custom-call | tf_op jit(solution)/shard_map/pallas_call | solution.py:349
  8.6 18.7 %all_to_all.20.arrived_ref = bf16[16,32,128]{2,1,0:T(8,128)(2,1)S(1)} all-to-all(bf16[16,32,128]{2,1,0:T(8,128)(2,1)S(1)} %get-tuple-element.8), channel_id=1, replica_groups=mesh['y'=4,'x'=4,'z'=8,'c'=2] {'z','c'}, dimensions={0} | all-to-all | bytes 262144 | tf_op jit(solution)/shard_map/all_to_all | solution.py:295
  27.2 0.0 copy-done.3
  27.2 0.3 shard_map.204
  27.6 20.8 %all_to_all.21 = bf16[128,4,128]{2,1,0:T(4,128)(2,1)S(1)} all-to-all(bf16[128,4,128]{2,1,0:T(4,128)(2,1)S(1)} %bitcast.28), channel_id=1, replica_groups=mesh['y'=4,'x'=4,'z'=8,'c'=2] {'y','x','z'}, dimensions={0} | all-to-all | bytes 262144 | tf_op jit(solution)/shard_map/all_to_all | solution.py:295
  48.4 1.7 %collective-permute-start = (bf16[512,128]{1,0:T(8,128)(2,1)S(1)}, bf16[512,128]{1,0:T(8,128)(2,1)S(1)}, u32[]{:S(2)}, u32[]{:S(2)}) collective-permute-start(bf16[512,128]{1,0:T(8,128)(2,1)S(1)} %bitcast.23), channel_id=1, source_target_pairs={{0,1},{1,0},{2,3},{3,2},{4,5},{5,4},{6,7},{7,6},{8,9},{9,8},{10,11... | collective-permute-start | bytes 393224 | tf_op jit(solution)/shard_map/ppermute | solution.py:389
  50.1 1.0 %collective-permute-done.theirs_ref = bf16[512,128]{1,0:T(8,128)(2,1)S(1)} collective-permute-done((bf16[512,128]{1,0:T(8,128)(2,1)S(1)}, bf16[512,128]{1,0:T(8,128)(2,1)S(1)}, u32[]{:S(2)}, u32[]{:S(2)}) %collective-permute-start) | collective-permute-done | bytes 131104 | tf_op jit(solution)/shard_map/ppermute | solution.py:389
  51.1 0.0 copy-done.1
  51.2 1.5 %shard_map.205 = (f32[512,128]{1,0:T(8,128)S(1)}, bf16[512,128]{1,0:T(8,128)(2,1)S(1)}) custom-call(s32[1]{0:T(128)} %bitcast.core_ref, bf16[512,128]{1,0:T(8,128)(2,1)S(1)} %bitcast.24, bf16[512,128]{1,0:T(8,128)(2,1)S(1)} %collective-permute-done.theirs_ref, f32[1,2048]{1,0:T(1,128)S(1)} %bitcast.31, bf16[1,2048,256]{2,1,0:T(8,128)(2,1)S(1)} %copy-done, ...), custom_call_target="tpu_custom_call" | custom-call | tf_op jit(solution)/shard_map/pallas_call | solution.py:390
  52.7 0.5 collective-permute-start.1
  53.1 1.0 %collective-permute-done.1 = bf16[512,128]{1,0:T(8,128)(2,1)S(1)} collective-permute-done((bf16[512,128]{1,0:T(8,128)(2,1)S(1)}, bf16[512,128]{1,0:T(8,128)(2,1)S(1)}, u32[]{:S(2)}, u32[]{:S(2)}) %collective-permute-start.1) | collective-permute-done | bytes 131104 | tf_op jit(solution)/shard_map/ppermute | solution.py:407
  54.2 17.2 %all_to_all.22 = bf16[128,4,128]{2,1,0:T(4,128)(2,1)S(1)} all-to-all(bf16[128,4,128]{2,1,0:T(4,128)(2,1)S(1)} %bitcast.33), channel_id=1, replica_groups=mesh['y'=4,'x'=4,'z'=8,'c'=2] {'y','x','z'}, dimensions={0} | all-to-all | bytes 262144 | tf_op jit(solution)/shard_map/all_to_all | solution.py:295
  71.4 0.3 shard_map.206
  71.7 13.1 %all_to_all.23 = bf16[16,32,128]{2,1,0:T(8,128)(2,1)S(1)} all-to-all(bf16[16,32,128]{2,1,0:T(8,128)(2,1)S(1)} %shard_map.206), channel_id=1, replica_groups=mesh['y'=4,'x'=4,'z'=8,'c'=2] {'z','c'}, dimensions={0} | all-to-all | bytes 262144 | tf_op jit(solution)/shard_map/all_to_all | solution.py:295
  84.8 0.7 copy_bitcast_fusion
  (10 shorter events, 0.0 us)
Async XLA Ops:
  0.6 26.6 %copy-start.3 = (bf16[32,2048]{1,0:T(8,128)(2,1)S(1)}, bf16[32,2048]{1,0:T(8,128)(2,1)}, u32[]{:S(2)}) copy-start(bf16[32,2048]{1,0:T(8,128)(2,1)} %layer_ref.1) | copy-start | bytes 393220
  0.6 26.6 %copy-start.7 = (s32[32,6]{0,1:T(8,128)S(1)}, s32[32,6]{0,1:T(8,128)}, u32[]{:S(2)}) copy-start(s32[32,6]{0,1:T(8,128)} %param.32) | copy-start | bytes 2308
  0.7 50.5 %copy-start.2 = (bf16[1,256,2048]{2,1,0:T(8,128)(2,1)S(1)}, bf16[1,256,2048]{2,1,0:T(8,128)(2,1)}, u32[]{:S(2)}) copy-start(bf16[1,256,2048]{2,1,0:T(8,128)(2,1)} %down_ref.1) | copy-start | bytes 3145732
  0.7 50.5 %copy-start.1 = (bf16[1,2048,256]{2,1,0:T(8,128)(2,1)S(1)}, bf16[1,2048,256]{2,1,0:T(8,128)(2,1)}, u32[]{:S(2)}) copy-start(bf16[1,2048,256]{2,1,0:T(8,128)(2,1)} %up_ref.1) | copy-start | bytes 3145732
  0.7 50.4 %copy-start = (bf16[1,2048,256]{2,1,0:T(8,128)(2,1)S(1)}, bf16[1,2048,256]{2,1,0:T(8,128)(2,1)}, u32[]{:S(2)}) copy-start(bf16[1,2048,256]{2,1,0:T(8,128)(2,1)} %gate_ref.1) | copy-start | bytes 3145732
  0.7 50.4 %copy-start.5 = (bf16[2048,32]{0,1:T(8,128)(2,1)S(1)}, bf16[2048,32]{0,1:T(8,128)(2,1)}, u32[]{:S(2)}) copy-start(bf16[2048,32]{0,1:T(8,128)(2,1)} %param.35) | copy-start | bytes 393220
  0.7 50.4 %copy-start.4 = (bf16[2048,32]{0,1:T(8,128)(2,1)S(1)}, bf16[2048,32]{0,1:T(8,128)(2,1)}, u32[]{:S(2)}) copy-start(bf16[2048,32]{0,1:T(8,128)(2,1)} %param.34) | copy-start | bytes 393220
  0.7 50.4 %copy-start.8 = (f32[2048]{0:T(1024)S(1)}, f32[2048]{0:T(1024)}, u32[]{:S(2)}) copy-start(f32[2048]{0:T(1024)} %param.31) | copy-start | bytes 24580
  0.7 70.6 %copy-start.9 = (f32[32,6]{0,1:T(8,128)S(1)}, f32[32,6]{0,1:T(8,128)}, u32[]{:S(2)}) copy-start(f32[32,6]{0,1:T(8,128)} %param.33) | copy-start | bytes 2308
  0.7 50.4 %copy-start.6 = (bf16[32,2048]{1,0:T(8,128)(2,1)S(1)}, bf16[32,2048]{1,0:T(8,128)(2,1)}, u32[]{:S(2)}) copy-start(bf16[32,2048]{1,0:T(8,128)(2,1)} %sdown_ref.1) | copy-start | bytes 393220
  48.4 2.7 %collective-permute-start = (bf16[512,128]{1,0:T(8,128)(2,1)S(1)}, bf16[512,128]{1,0:T(8,128)(2,1)S(1)}, u32[]{:S(2)}, u32[]{:S(2)}) collective-permute-start(bf16[512,128]{1,0:T(8,128)(2,1)S(1)} %bitcast.23), channel_id=1, source_target_pairs={{0,1},{1,0},{2,3},{3,2},{4,5},{5,4},{6,7},{7,6},{8,9},{9,8},{10,11... | collective-permute-start | bytes 393224 | tf_op jit(solution)/shard_map/ppermute | solution.py:389
  52.7 1.4 %collective-permute-start.1 = (bf16[512,128]{1,0:T(8,128)(2,1)S(1)}, bf16[512,128]{1,0:T(8,128)(2,1)S(1)}, u32[]{:S(2)}, u32[]{:S(2)}) collective-permute-start(bf16[512,128]{1,0:T(8,128)(2,1)S(1)} %get-tuple-element.11), channel_id=1, source_target_pairs={{0,1},{1,0},{2,3},{3,2},{4,5},{5,4},{6,7},{7,6},{8,9},{9,8},{10,11... | collective-permute-start | bytes 393224 | tf_op jit(solution)/shard_map/ppermute | solution.py:407

commit v7 on v6

--- a/solution.py
+++ b/solution.py
@@ -57,7 +57,6 @@
     layer_ref,
     gain_ref,
     first_ref,
-    second_ref,
     wo_ref,
     cum_ref,
     score_ref,
@@ -73,9 +72,9 @@
         (gain_hbm, gain_ref),
         (wq_hbm, first_ref.at[:hd]),
         (wk_hbm, first_ref.at[hd : 2 * hd]),
-        (wf_hbm, first_ref.at[2 * hd :]),
+        (wv_hbm, first_ref.at[2 * hd : 3 * hd]),
+        (wf_hbm, first_ref.at[3 * hd :]),
         (cum_hbm, cum_ref),
-        (wv_hbm, second_ref),
         (wo_hbm, wo_ref),
         (lengths_hbm, lengths_ref),
         (bias_hbm, bias_ref),
@@ -95,7 +94,7 @@
         copy.start()
     lax.fori_loop(0, rows, start, 0)
 
-    for copy in small[:5] + small[8:]:
+    for copy in small[:6] + small[8:]:
         copy.wait()
     lane = lax.broadcasted_iota(jnp.int32, (1, LANES), 1)
     length = jnp.zeros((1, LANES), jnp.int32)
@@ -114,11 +113,11 @@
     head = head_ref[0]
     head_row = lax.broadcasted_iota(jnp.int32, (gates, LANES), 0) == head
     logit = (
-        jnp.sum(jnp.where(head_row, by_seq[2 * hd :], 0.0), axis=0, keepdims=True) + bias_ref[head]
+        jnp.sum(jnp.where(head_row, by_seq[3 * hd :], 0.0), axis=0, keepdims=True) + bias_ref[head]
     )
     forget = -(jnp.maximum(-logit, 0.0) + jnp.log1p(jnp.exp(-jnp.abs(logit))))
 
-    small[5].wait()
+    small[6].wait()
     cum = cum_ref[...].reshape(rows, span)
     cum = jnp.concatenate([cum, jnp.zeros((LANES - rows, span), F32)], axis=0)
     cum = jnp.transpose(cum)
@@ -126,10 +125,7 @@
     latest = jnp.sum(jnp.where(position == length - 1, cum, 0.0), axis=0, keepdims=True)
     shift = (latest + forget) - cum
 
-    for copy in small[6:8]:
-        copy.wait()
-    new_kv = nt(normed, jnp.concatenate([first_ref[hd : 2 * hd], second_ref[...]], axis=0))
-    new_kv = new_kv.astype(BF)
+    new_kv = jnp.transpose(by_seq[hd : 3 * hd])[:rows].astype(BF)
     newkv_ref[...] = new_kv
     query = jnp.concatenate([query, jnp.zeros((LANES - hd, LANES), F32)], axis=0)
     lane_full = lax.broadcasted_iota(jnp.int32, (LANES, LANES), 1)
@@ -163,19 +159,20 @@
         jnp.where(square_row == square_lane, own, 0.0), axis=1, keepdims=True
     )
     blended = own_column * new_kv.astype(F32)
-    step = 16
-
-    def value_step(i, total):
-        for k in range(step):
-            s = (i * step + k) * 2
-            at = pl.multiple_of(s * LANES, LANES)
-            two = mm(probs, kv_buf[:, pl.ds(at, 2 * LANES)])
-            total = total + jnp.where(square_row == s, two[:, :LANES], 0.0)
-            total = total + jnp.where(square_row == s + 1, two[:, LANES:], 0.0)
-        return total
-
-    blended = lax.fori_loop(0, rows // (2 * step), value_step, blended)
+    half = rows // 2
+    parts = []
+    for h in range(0, rows, half):
+        some = probs[h : h + half]
+        mark = lax.broadcasted_iota(jnp.int32, (half, LANES), 0) + h
+        total = blended[h : h + half]
+        for s in range(h, h + half, 2):
+            two = mm(some, kv_buf[:, s * LANES : (s + 2) * LANES])
+            total = total + jnp.where(mark == s, two[:, :LANES], 0.0)
+            total = total + jnp.where(mark == s + 1, two[:, LANES:], 0.0)
+        parts.append(total)
+    blended = jnp.concatenate(parts, axis=0)
     attended = blended[:, hd:].astype(BF)
+    small[7].wait()
     out = mm(attended, wo_ref[...])
     for t in range(part_ref.shape[0]):
         part_ref[t] = out[:, t * LANES : (t + 1) * LANES].astype(BF)
@@ -356,8 +353,7 @@
             pltpu.SMEM((gates,), F32),
             VMEM((rows, width), BF),
             VMEM((1, width), F32),
-            VMEM((2 * hd + gates, width), BF),
-            VMEM((hd, width), BF),
+            VMEM((3 * hd + gates, width), BF),
             VMEM((hd, width), BF),
             VMEM((rows, 1, span), F32),
             VMEM((span, LANES), F32),

time: 85.7 us -> 85.4 us (level)
  no operation moved by 1% of the time
where the time goes in v7:
time: 85.4 us; the launch traced here: 85.2 us
  blocking collectives  69.8 us (82%)
  Pallas kernels  9.7 us (11%)
  starting transfers between devices  2.18 us (3%)
  waiting for transfers between devices  1.97 us (2%)
    all_to_all x4, blocking collectives, exchange(): return lax.all_to_all(x, axes, split_axis=0, concat_axis=0, tiled=True)  69.8 us
    pallas_call x1, Pallas kernels, body(): call(attention_kernel, [shape((tp_count, rows, LANES), BF), shape((rows,...  7.52 us
    ppermute x1, starting transfers between devices, body(): theirs = lax.ppermute(mine, 'c', SWAP)  1.72 us
  transfers between devices with their start and end apart: 2, of which 2 were waited for; matrix products, arithmetic and copies ran while one was open for 0% of the time, Pallas kernels for 0%

profile of v7, /device:TPU:1, one launch (start us, length us, event | category | flops | bytes accessed | tf_op | source)
XLA Modules:
  0.0 85.2 jit_solution(17601740039682714457)
XLA Ops:
  0.6 0.0 copy-start.3
  0.6 0.0 copy-start.7
  0.7 0.0 copy-start.2
  0.7 0.0 copy-start.1
  0.7 0.0 copy-start
  0.7 0.0 copy-start.5
  0.7 0.0 copy-start.4
  0.7 0.0 copy-start.8
  0.7 0.0 copy-start.9
  0.7 0.0 copy-start.6
  0.7 7.5 %shard_map.203 = (bf16[16,32,128]{2,1,0:T(8,128)(2,1)S(1)}, bf16[32,128]{1,0:T(8,128)(2,1)}) custom-call(s32[32]{0:T(128)} %lengths_hbm.1, f32[16]{0:T(128)} %bias_hbm.1, s32[1]{0:T(128)} %bitcast.1.head_ref.tp_ref, bf16[32,2048]{1,0:T(8,128)(2,1)} %layer_ref.1, f32[1,2048]{1,0:T(1,128)} %bitcast.38, bf16[64,2048]{1,0:T(8,128)(2,1)} %bitcast.34, ...), custom_call_target="tpu_custom_call" | custom-call | tf_op jit(solution)/shard_map/pallas_call | solution.py:346
  8.3 18.6 %all_to_all.20.arrived_ref = bf16[16,32,128]{2,1,0:T(8,128)(2,1)S(1)} all-to-all(bf16[16,32,128]{2,1,0:T(8,128)(2,1)S(1)} %get-tuple-element.8), channel_id=1, replica_groups=mesh['y'=4,'x'=4,'z'=8,'c'=2] {'z','c'}, dimensions={0} | all-to-all | bytes 262144 | tf_op jit(solution)/shard_map/all_to_all | solution.py:292
  26.9 0.0 copy-done.3
  26.9 0.3 shard_map.204
  27.3 20.8 %all_to_all.21 = bf16[128,4,128]{2,1,0:T(4,128)(2,1)S(1)} all-to-all(bf16[128,4,128]{2,1,0:T(4,128)(2,1)S(1)} %bitcast.28), channel_id=1, replica_groups=mesh['y'=4,'x'=4,'z'=8,'c'=2] {'y','x','z'}, dimensions={0} | all-to-all | bytes 262144 | tf_op jit(solution)/shard_map/all_to_all | solution.py:292
  48.1 1.7 %collective-permute-start = (bf16[512,128]{1,0:T(8,128)(2,1)S(1)}, bf16[512,128]{1,0:T(8,128)(2,1)S(1)}, u32[]{:S(2)}, u32[]{:S(2)}) collective-permute-start(bf16[512,128]{1,0:T(8,128)(2,1)S(1)} %bitcast.23), channel_id=1, source_target_pairs={{0,1},{1,0},{2,3},{3,2},{4,5},{5,4},{6,7},{7,6},{8,9},{9,8},{10,11... | collective-permute-start | bytes 393224 | tf_op jit(solution)/shard_map/ppermute | solution.py:385
  49.8 1.0 %collective-permute-done.theirs_ref = bf16[512,128]{1,0:T(8,128)(2,1)S(1)} collective-permute-done((bf16[512,128]{1,0:T(8,128)(2,1)S(1)}, bf16[512,128]{1,0:T(8,128)(2,1)S(1)}, u32[]{:S(2)}, u32[]{:S(2)}) %collective-permute-start) | collective-permute-done | bytes 131104 | tf_op jit(solution)/shard_map/ppermute | solution.py:385
  50.8 1.5 %shard_map.205 = (f32[512,128]{1,0:T(8,128)S(1)}, bf16[512,128]{1,0:T(8,128)(2,1)S(1)}) custom-call(s32[1]{0:T(128)} %bitcast.core_ref, bf16[512,128]{1,0:T(8,128)(2,1)S(1)} %bitcast.24, bf16[512,128]{1,0:T(8,128)(2,1)S(1)} %collective-permute-done.theirs_ref, f32[1,2048]{1,0:T(1,128)S(1)} %bitcast.31, bf16[1,2048,256]{2,1,0:T(8,128)(2,1)S(1)} %copy-done, ...), custom_call_target="tpu_custom_call" | custom-call | tf_op jit(solution)/shard_map/pallas_call | solution.py:386
  52.4 0.5 collective-permute-start.1
  52.8 1.0 %collective-permute-done.1 = bf16[512,128]{1,0:T(8,128)(2,1)S(1)} collective-permute-done((bf16[512,128]{1,0:T(8,128)(2,1)S(1)}, bf16[512,128]{1,0:T(8,128)(2,1)S(1)}, u32[]{:S(2)}, u32[]{:S(2)}) %collective-permute-start.1) | collective-permute-done | bytes 131104 | tf_op jit(solution)/shard_map/ppermute | solution.py:403
  53.8 17.2 %all_to_all.22 = bf16[128,4,128]{2,1,0:T(4,128)(2,1)S(1)} all-to-all(bf16[128,4,128]{2,1,0:T(4,128)(2,1)S(1)} %bitcast.33), channel_id=1, replica_groups=mesh['y'=4,'x'=4,'z'=8,'c'=2] {'y','x','z'}, dimensions={0} | all-to-all | bytes 262144 | tf_op jit(solution)/shard_map/all_to_all | solution.py:292
  71.0 0.3 shard_map.206
  71.4 13.1 %all_to_all.23 = bf16[16,32,128]{2,1,0:T(8,128)(2,1)S(1)} all-to-all(bf16[16,32,128]{2,1,0:T(8,128)(2,1)S(1)} %shard_map.206), channel_id=1, replica_groups=mesh['y'=4,'x'=4,'z'=8,'c'=2] {'z','c'}, dimensions={0} | all-to-all | bytes 262144 | tf_op jit(solution)/shard_map/all_to_all | solution.py:292
  84.5 0.7 copy_bitcast_fusion
  (10 shorter events, 0.0 us)
Async XLA Ops:
  0.6 26.3 %copy-start.3 = (bf16[32,2048]{1,0:T(8,128)(2,1)S(1)}, bf16[32,2048]{1,0:T(8,128)(2,1)}, u32[]{:S(2)}) copy-start(bf16[32,2048]{1,0:T(8,128)(2,1)} %layer_ref.1) | copy-start | bytes 393220
  0.6 26.3 %copy-start.7 = (s32[32,6]{0,1:T(8,128)S(1)}, s32[32,6]{0,1:T(8,128)}, u32[]{:S(2)}) copy-start(s32[32,6]{0,1:T(8,128)} %param.32) | copy-start | bytes 2308
  0.7 50.1 %copy-start.2 = (bf16[1,256,2048]{2,1,0:T(8,128)(2,1)S(1)}, bf16[1,256,2048]{2,1,0:T(8,128)(2,1)}, u32[]{:S(2)}) copy-start(bf16[1,256,2048]{2,1,0:T(8,128)(2,1)} %down_ref.1) | copy-start | bytes 3145732
  0.7 50.1 %copy-start.1 = (bf16[1,2048,256]{2,1,0:T(8,128)(2,1)S(1)}, bf16[1,2048,256]{2,1,0:T(8,128)(2,1)}, u32[]{:S(2)}) copy-start(bf16[1,2048,256]{2,1,0:T(8,128)(2,1)} %up_ref.1) | copy-start | bytes 3145732
  0.7 50.1 %copy-start = (bf16[1,2048,256]{2,1,0:T(8,128)(2,1)S(1)}, bf16[1,2048,256]{2,1,0:T(8,128)(2,1)}, u32[]{:S(2)}) copy-start(bf16[1,2048,256]{2,1,0:T(8,128)(2,1)} %gate_ref.1) | copy-start | bytes 3145732
  0.7 50.1 %copy-start.5 = (bf16[2048,32]{0,1:T(8,128)(2,1)S(1)}, bf16[2048,32]{0,1:T(8,128)(2,1)}, u32[]{:S(2)}) copy-start(bf16[2048,32]{0,1:T(8,128)(2,1)} %param.35) | copy-start | bytes 393220
  0.7 50.1 %copy-start.4 = (bf16[2048,32]{0,1:T(8,128)(2,1)S(1)}, bf16[2048,32]{0,1:T(8,128)(2,1)}, u32[]{:S(2)}) copy-start(bf16[2048,32]{0,1:T(8,128)(2,1)} %param.34) | copy-start | bytes 393220
  0.7 50.1 %copy-start.8 = (f32[2048]{0:T(1024)S(1)}, f32[2048]{0:T(1024)}, u32[]{:S(2)}) copy-start(f32[2048]{0:T(1024)} %param.31) | copy-start | bytes 24580
  0.7 70.3 %copy-start.9 = (f32[32,6]{0,1:T(8,128)S(1)}, f32[32,6]{0,1:T(8,128)}, u32[]{:S(2)}) copy-start(f32[32,6]{0,1:T(8,128)} %param.33) | copy-start | bytes 2308
  0.7 50.1 %copy-start.6 = (bf16[32,2048]{1,0:T(8,128)(2,1)S(1)}, bf16[32,2048]{1,0:T(8,128)(2,1)}, u32[]{:S(2)}) copy-start(bf16[32,2048]{1,0:T(8,128)(2,1)} %sdown_ref.1) | copy-start | bytes 393220
  48.1 2.7 %collective-permute-start = (bf16[512,128]{1,0:T(8,128)(2,1)S(1)}, bf16[512,128]{1,0:T(8,128)(2,1)S(1)}, u32[]{:S(2)}, u32[]{:S(2)}) collective-permute-start(bf16[512,128]{1,0:T(8,128)(2,1)S(1)} %bitcast.23), channel_id=1, source_target_pairs={{0,1},{1,0},{2,3},{3,2},{4,5},{5,4},{6,7},{7,6},{8,9},{9,8},{10,11... | collective-permute-start | bytes 393224 | tf_op jit(solution)/shard_map/ppermute | solution.py:385
  52.4 1.4 %collective-permute-start.1 = (bf16[512,128]{1,0:T(8,128)(2,1)S(1)}, bf16[512,128]{1,0:T(8,128)(2,1)S(1)}, u32[]{:S(2)}, u32[]{:S(2)}) collective-permute-start(bf16[512,128]{1,0:T(8,128)(2,1)S(1)} %get-tuple-element.11), channel_id=1, source_target_pairs={{0,1},{1,0},{2,3},{3,2},{4,5},{5,4},{6,7},{7,6},{8,9},{9,8},{10,11... | collective-permute-start | bytes 393224 | tf_op jit(solution)/shard_map/ppermute | solution.py:403

commit v8 on v7

--- a/solution.py
+++ b/solution.py
@@ -220,56 +220,99 @@
     send_ref[...] = tn(place, middle).astype(BF)
 
 
+GROUPS = 16
+KINDS = 4
+
+
+def side_products(side, arrived, wide_ref, gain_ref, gate_ref, up_ref, sgate_ref, sup_ref):
+    stride = arrived.shape[0] // GROUPS
+    tiles = stride // KINDS
+    wide_ref[...] = arrived.astype(F32)
+    rows = jnp.concatenate(
+        [
+            jnp.concatenate(
+                [wide_ref[pl.ds(t * KINDS + s, GROUPS, stride=stride), :] for t in range(tiles)],
+                axis=1,
+            )
+            for s in range(KINDS)
+        ],
+        axis=0,
+    )
+    spans = [
+        pl.ds(pl.multiple_of((2 * t + side) * LANES, LANES), LANES) for t in range(tiles)
+    ]
+    gain = jnp.concatenate([gain_ref[:, at] for at in spans], axis=1)
+    squares = jnp.sum(rows * rows, axis=1, keepdims=True)
+    scaled = (rows * gain).astype(BF)
+    half = scaled.shape[0] // 2
+    routed, shared = scaled[:half], scaled[half:]
+    return (
+        squares,
+        mm(routed, jnp.concatenate([gate_ref[0, at, :] for at in spans], axis=0)),
+        mm(routed, jnp.concatenate([up_ref[0, at, :] for at in spans], axis=0)),
+        nt(shared, jnp.concatenate([sgate_ref[:, at] for at in spans], axis=1)),
+        nt(shared, jnp.concatenate([sup_ref[:, at] for at in spans], axis=1)),
+    )
+
+
+def own_kernel(core_ref, mine_ref, *refs):
+    weights, (squares_ref, *outs), wide_ref = refs[:5], refs[5:10], refs[10]
+    squares, *products = side_products(core_ref[0], mine_ref[...], wide_ref, *weights)
+    squares_ref[...] = jnp.broadcast_to(squares, squares_ref.shape)
+    for ref, product in zip(outs, products):
+        ref[...] = product
+
+
 def expert_kernel(
     core_ref,
-    mine_ref,
     theirs_ref,
+    squares_ref,
+    g_ref,
+    u_ref,
+    sg_ref,
+    su_ref,
     gain_ref,
     gate_ref,
     up_ref,
-    down_ref,
     sgate_ref,
     sup_ref,
+    down_ref,
     sdown_ref,
     keep_ref,
     give_ref,
     even_ref,
     odd_ref,
 ):
-    groups = 16
-    kinds = 4
-    stride = mine_ref.shape[0] // groups
-    tiles = stride // kinds
     first = core_ref[0] == 0
-    mine = mine_ref[...].astype(F32)
-    theirs = theirs_ref[...].astype(F32)
-    even_ref[...] = jnp.where(first, mine, theirs)
-    odd_ref[...] = jnp.where(first, theirs, mine)
-    sides = (even_ref, odd_ref)
-
-    def rows_of(s):
-        return jnp.concatenate(
-            [
-                sides[t % 2][pl.ds((t // 2) * kinds + s, groups, stride=stride), :]
-                for t in range(2 * tiles)
-            ],
-            axis=1,
-        )
+    squares, g, u, sg, su = side_products(
+        1 - core_ref[0],
+        theirs_ref[...],
+        even_ref,
+        gain_ref,
+        gate_ref,
+        up_ref,
+        sgate_ref,
+        sup_ref,
+    )
+    width = gain_ref.shape[1]
+    squares = squares + squares_ref[:, :1]
+    factor = lax.rsqrt(squares / width + NORM_EPS)
+    half = factor.shape[0] // 2
 
     def swish(v):
         return v / (1.0 + jnp.exp(-v))
 
-    gain = gain_ref[...]
-    routed = rms_rows(jnp.concatenate([rows_of(0), rows_of(1)], axis=0), gain)
-    shared = rms_rows(jnp.concatenate([rows_of(2), rows_of(3)], axis=0), gain)
-    hidden = (swish(mm(routed, gate_ref[0])) * mm(routed, up_ref[0])).astype(BF)
+    fr, fs = factor[:half], factor[half:]
+    hidden = (swish((g + g_ref[...]) * fr) * ((u + u_ref[...]) * fr)).astype(BF)
     served = mm(hidden, down_ref[0])
-    shidden = (swish(nt(shared, sgate_ref[...])) * nt(shared, sup_ref[...])).astype(BF)
+    shidden = (swish((sg + sg_ref[...]) * fs) * ((su + su_ref[...]) * fs)).astype(BF)
     sserved = mm(shidden, sdown_ref[...])
+    sides = (even_ref, odd_ref)
+    stride = theirs_ref.shape[0] // GROUPS
     for s, block in enumerate((served, served, sserved, sserved)):
-        for t in range(2 * tiles):
-            sides[t % 2][pl.ds((t // 2) * kinds + s, groups, stride=stride), :] = block[
-                (s % 2) * groups : (s % 2 + 1) * groups, t * LANES : (t + 1) * LANES
+        for t in range(width // LANES):
+            sides[t % 2][pl.ds((t // 2) * KINDS + s, GROUPS, stride=stride), :] = block[
+                (s % 2) * GROUPS : (s % 2 + 1) * GROUPS, t * LANES : (t + 1) * LANES
             ]
     even = even_ref[...]
     odd = odd_ref[...]
@@ -383,23 +426,30 @@
     )(tp, arrived, layer_in, ids)
     mine = exchange(send.reshape(chips, 4, LANES), CHIPS).reshape(slots, LANES)
     theirs = lax.ppermute(mine, "c", SWAP)
+    sff = shared_gate.shape[1]
+    eff = expert_gate.shape[2]
+    weights = (
+        ffn_gain.reshape(1, width),
+        expert_gate,
+        expert_up,
+        shared_gate.T,
+        shared_up.T,
+    )
+    wide = VMEM((slots, LANES), F32)
+    own = call(
+        own_kernel,
+        [shape((2 * rows, LANES), F32)]
+        + [shape((rows, eff), F32)] * 2
+        + [shape((rows, sff), F32)] * 2,
+        in_specs=[smem] + [vmem] * 6,
+        scratch=[wide],
+    )(core, mine, *weights)
     keep, give = call(
         expert_kernel,
         [shape((slots, LANES), F32), shape((slots, LANES), BF)],
-        in_specs=[smem] + [vmem] * 9,
-        scratch=[VMEM((slots, LANES), F32)] * 2,
-    )(
-        core,
-        mine,
-        theirs,
-        ffn_gain.reshape(1, width),
-        expert_gate,
-        expert_up,
-        expert_down,
-        shared_gate.T,
-        shared_up.T,
-        shared_down,
-    )
+        in_specs=[smem] + [vmem] * 13,
+        scratch=[wide, wide],
+    )(core, theirs, *own, *weights, expert_down, shared_down)
     send = (keep + lax.ppermute(give, "c", SWAP).astype(F32)).astype(BF)
     arrived = exchange(send.reshape(chips, 4, LANES), CHIPS).reshape(slots, LANES)
     send = call(

time: 85.4 us -> 84.9 us (level)
  no operation moved by 1% of the time
where the time goes in v8:
time: 84.9 us; the launch traced here: 84.7 us
  blocking collectives  69.8 us (82%)
  Pallas kernels  9.65 us (11%)
  starting transfers between devices  2.17 us (3%)
  waiting for transfers between devices  1.57 us (2%)
    all_to_all x4, blocking collectives, exchange(): return lax.all_to_all(x, axes, split_axis=0, concat_axis=0, tiled=True)  69.8 us
    pallas_call x1, Pallas kernels, body(): call(attention_kernel, [shape((tp_count, rows, LANES), BF), shape((rows,...  7.49 us
    ppermute x1, starting transfers between devices, body(): theirs = lax.ppermute(mine, 'c', SWAP)  1.72 us
  transfers between devices with their start and end apart: 2, of which 2 were waited for; matrix products, arithmetic and copies ran while one was open for 0% of the time, Pallas kernels for 0%

profile of v8, /device:TPU:1, one launch (start us, length us, event | category | flops | bytes accessed | tf_op | source)
XLA Modules:
  0.0 84.7 jit_solution(4635188935566343409)
XLA Ops:
  0.6 0.0 copy-start.3
  0.6 0.0 copy-start.8
  0.7 0.0 copy-start.1
  0.7 0.0 copy-start
  0.7 0.0 copy-start.5
  0.7 0.0 copy-start.4
  0.7 0.0 copy-start.7
  0.7 0.0 copy-start.2
  0.7 7.5 %shard_map.203 = (bf16[16,32,128]{2,1,0:T(8,128)(2,1)S(1)}, bf16[32,128]{1,0:T(8,128)(2,1)}) custom-call(s32[32]{0:T(128)} %lengths_hbm.1, f32[16]{0:T(128)} %bias_hbm.1, s32[1]{0:T(128)} %bitcast.1.head_ref.tp_ref, bf16[32,2048]{1,0:T(8,128)(2,1)} %layer_ref.1, f32[1,2048]{1,0:T(1,128)} %bitcast.41, bf16[64,2048]{1,0:T(8,128)(2,1)} %bitcast.37, ...), custom_call_target="tpu_custom_call" | custom-call | tf_op jit(solution)/shard_map/pallas_call | solution.py:389
  8.2 18.7 %all_to_all.20.arrived_ref = bf16[16,32,128]{2,1,0:T(8,128)(2,1)S(1)} all-to-all(bf16[16,32,128]{2,1,0:T(8,128)(2,1)S(1)} %get-tuple-element.13), channel_id=1, replica_groups=mesh['y'=4,'x'=4,'z'=8,'c'=2] {'z','c'}, dimensions={0} | all-to-all | bytes 262144 | tf_op jit(solution)/shard_map/all_to_all | solution.py:335
  26.9 0.3 shard_map.204
  27.3 20.8 %all_to_all.21 = bf16[128,4,128]{2,1,0:T(4,128)(2,1)S(1)} all-to-all(bf16[128,4,128]{2,1,0:T(4,128)(2,1)S(1)} %bitcast.30), channel_id=1, replica_groups=mesh['y'=4,'x'=4,'z'=8,'c'=2] {'y','x','z'}, dimensions={0} | all-to-all | bytes 262144 | tf_op jit(solution)/shard_map/all_to_all | solution.py:335
  48.1 1.7 %collective-permute-start = (bf16[512,128]{1,0:T(8,128)(2,1)S(1)}, bf16[512,128]{1,0:T(8,128)(2,1)S(1)}, u32[]{:S(2)}, u32[]{:S(2)}) collective-permute-start(bf16[512,128]{1,0:T(8,128)(2,1)S(1)} %bitcast.27), channel_id=1, source_target_pairs={{0,1},{1,0},{2,3},{3,2},{4,5},{5,4},{6,7},{7,6},{8,9},{9,8},{10,11... | collective-permute-start | bytes 393224 | tf_op jit(solution)/shard_map/ppermute | solution.py:428
  49.8 0.0 copy-done
  49.8 0.0 copy-done.4
  49.8 0.4 shard_map.205
  50.2 0.6 collective-permute-done.theirs_ref
  50.8 1.1 %shard_map.206 = (f32[512,128]{1,0:T(8,128)S(1)}, bf16[512,128]{1,0:T(8,128)(2,1)S(1)}) custom-call(s32[1]{0:T(128)} %bitcast.core_ref, bf16[512,128]{1,0:T(8,128)(2,1)S(1)} %collective-permute-done.theirs_ref, f32[64,128]{1,0:T(8,128)S(1)} %get-tuple-element.15.squares_ref, f32[32,256]{1,0:T(8,128)S(1)} %get-tuple-element.16.g_ref, ...), custom_call_target="tpu_custom_call" | custom-call | tf_op jit(solution)/shard_map/pallas_call | solution.py:447
  51.9 0.4 collective-permute-start.1
  52.3 1.0 %collective-permute-done.1 = bf16[512,128]{1,0:T(8,128)(2,1)S(1)} collective-permute-done((bf16[512,128]{1,0:T(8,128)(2,1)S(1)}, bf16[512,128]{1,0:T(8,128)(2,1)S(1)}, u32[]{:S(2)}, u32[]{:S(2)}) %collective-permute-start.1) | collective-permute-done | bytes 131104 | tf_op jit(solution)/shard_map/ppermute | solution.py:453
  53.4 17.2 %all_to_all.22 = bf16[128,4,128]{2,1,0:T(4,128)(2,1)S(1)} all-to-all(bf16[128,4,128]{2,1,0:T(4,128)(2,1)S(1)} %bitcast.36), channel_id=1, replica_groups=mesh['y'=4,'x'=4,'z'=8,'c'=2] {'y','x','z'}, dimensions={0} | all-to-all | bytes 262144 | tf_op jit(solution)/shard_map/all_to_all | solution.py:335
  70.6 0.3 shard_map.207
  70.9 13.1 %all_to_all.23 = bf16[16,32,128]{2,1,0:T(8,128)(2,1)S(1)} all-to-all(bf16[16,32,128]{2,1,0:T(8,128)(2,1)S(1)} %shard_map.207), channel_id=1, replica_groups=mesh['y'=4,'x'=4,'z'=8,'c'=2] {'z','c'}, dimensions={0} | all-to-all | bytes 262144 | tf_op jit(solution)/shard_map/all_to_all | solution.py:335
  84.0 0.7 copy_bitcast_fusion
  (11 shorter events, 0.1 us)
Async XLA Ops:
  0.6 26.3 %copy-start.3 = (bf16[32,2048]{1,0:T(8,128)(2,1)S(1)}, bf16[32,2048]{1,0:T(8,128)(2,1)}, u32[]{:S(2)}) copy-start(bf16[32,2048]{1,0:T(8,128)(2,1)} %layer_ref.1) | copy-start | bytes 393220
  0.6 26.3 %copy-start.8 = (s32[32,6]{0,1:T(8,128)S(1)}, s32[32,6]{0,1:T(8,128)}, u32[]{:S(2)}) copy-start(s32[32,6]{0,1:T(8,128)} %param.32) | copy-start | bytes 2308
  0.7 49.1 %copy-start.1 = (bf16[1,2048,256]{2,1,0:T(8,128)(2,1)S(1)}, bf16[1,2048,256]{2,1,0:T(8,128)(2,1)}, u32[]{:S(2)}) copy-start(bf16[1,2048,256]{2,1,0:T(8,128)(2,1)} %up_ref.1) | copy-start | bytes 3145732
  0.7 49.1 %copy-start = (bf16[1,2048,256]{2,1,0:T(8,128)(2,1)S(1)}, bf16[1,2048,256]{2,1,0:T(8,128)(2,1)}, u32[]{:S(2)}) copy-start(bf16[1,2048,256]{2,1,0:T(8,128)(2,1)} %gate_ref.1) | copy-start | bytes 3145732
  0.7 49.1 %copy-start.5 = (bf16[2048,32]{0,1:T(8,128)(2,1)S(1)}, bf16[2048,32]{0,1:T(8,128)(2,1)}, u32[]{:S(2)}) copy-start(bf16[2048,32]{0,1:T(8,128)(2,1)} %param.35) | copy-start | bytes 393220
  0.7 49.1 %copy-start.4 = (bf16[2048,32]{0,1:T(8,128)(2,1)S(1)}, bf16[2048,32]{0,1:T(8,128)(2,1)}, u32[]{:S(2)}) copy-start(bf16[2048,32]{0,1:T(8,128)(2,1)} %param.34) | copy-start | bytes 393220
  0.7 49.1 %copy-start.7 = (f32[2048]{0:T(1024)S(1)}, f32[2048]{0:T(1024)}, u32[]{:S(2)}) copy-start(f32[2048]{0:T(1024)} %param.31) | copy-start | bytes 24580
  0.7 50.1 %copy-start.2 = (bf16[1,256,2048]{2,1,0:T(8,128)(2,1)S(1)}, bf16[1,256,2048]{2,1,0:T(8,128)(2,1)}, u32[]{:S(2)}) copy-start(bf16[1,256,2048]{2,1,0:T(8,128)(2,1)} %down_ref.1) | copy-start | bytes 3145732
  0.7 50.0 %copy-start.6 = (bf16[32,2048]{1,0:T(8,128)(2,1)S(1)}, bf16[32,2048]{1,0:T(8,128)(2,1)}, u32[]{:S(2)}) copy-start(bf16[32,2048]{1,0:T(8,128)(2,1)} %sdown_ref.1) | copy-start | bytes 393220
  0.7 69.8 %copy-start.9 = (f32[32,6]{0,1:T(8,128)S(1)}, f32[32,6]{0,1:T(8,128)}, u32[]{:S(2)}) copy-start(f32[32,6]{0,1:T(8,128)} %param.33) | copy-start | bytes 2308
  48.1 2.7 %collective-permute-start = (bf16[512,128]{1,0:T(8,128)(2,1)S(1)}, bf16[512,128]{1,0:T(8,128)(2,1)S(1)}, u32[]{:S(2)}, u32[]{:S(2)}) collective-permute-start(bf16[512,128]{1,0:T(8,128)(2,1)S(1)} %bitcast.27), channel_id=1, source_target_pairs={{0,1},{1,0},{2,3},{3,2},{4,5},{5,4},{6,7},{7,6},{8,9},{9,8},{10,11... | collective-permute-start | bytes 393224 | tf_op jit(solution)/shard_map/ppermute | solution.py:428
  51.9 1.4 %collective-permute-start.1 = (bf16[512,128]{1,0:T(8,128)(2,1)S(1)}, bf16[512,128]{1,0:T(8,128)(2,1)S(1)}, u32[]{:S(2)}, u32[]{:S(2)}) collective-permute-start(bf16[512,128]{1,0:T(8,128)(2,1)S(1)} %get-tuple-element.21), channel_id=1, source_target_pairs={{0,1},{1,0},{2,3},{3,2},{4,5},{5,4},{6,7},{7,6},{8,9},{9,8},{10,11... | collective-permute-start | bytes 393224 | tf_op jit(solution)/shard_map/ppermute | solution.py:453
